TPU v7x, 128 devices: a whole 4x4x4 slice. The times are simulated.
128 devices in a mesh: sp: 16 (over z, y), fs: 4 (over x), tp: 2 (over core).
Axes of the slice: x: 4, y: 4, z: 4, core: 2. Of those that a mesh axis runs over, the one named last changes fastest.
Arguments:
- tokens: bfloat16 [8, 2048, 2048], P('fs', 'sp', 'tp'), may hold values from -8 to 8
- norm_gain: float32 [2048], replicated, may hold values from 0.1 to 1.9
- w_recept: bfloat16 [2048, 768], P(None, 'tp'), may hold values from -0.125 to 0.125
- w_key: bfloat16 [2048, 768], P(None, 'tp'), may hold values from -0.125 to 0.125
- w_value: bfloat16 [2048, 768], P(None, 'tp'), may hold values from -0.125 to 0.125
- w_decay: bfloat16 [2048, 768], P(None, 'tp'), may hold values from -0.125 to 0.125
- w_rate: bfloat16 [2048, 768], P(None, 'tp'), may hold values from -0.125 to 0.125
- w_gate_rec: bfloat16 [2048, 768], P(None, 'tp'), may hold values from -0.125 to 0.125
- w_pool: bfloat16 [2048, 512], P(None, 'tp'), may hold values from -0.125 to 0.125
- w_gate_pool: bfloat16 [2048, 512], P(None, 'tp'), may hold values from -0.125 to 0.125
- decay_base: float32 [768], replicated, may hold values from -12 to -2.5
- rate_base: float32 [768], replicated, may hold values from -7 to 1
- head_gain: float32 [768], replicated, may hold values from 0.1 to 1.9
- pool_mix: bfloat16 [4, 128, 128], replicated, may hold values from -0.5 to 0.5
- pool_scale: float32 [512], replicated, may hold values from 0.3 to 3
- w_out_rec: bfloat16 [768, 2048], P('tp'), may hold values from -0.15625 to 0.15625
- w_out_pool: bfloat16 [512, 2048], P('tp'), may hold values from -0.15625 to 0.15625
- init_state: float32 [8, 12, 64, 64], P('fs', 'tp'), may hold values from -240 to 240
Outputs:
- mixed: bfloat16 [8, 2048, 2048], P('fs', 'sp', 'tp')
All inputs are finite; a program needn't handle non-finite values.
Results may differ from a plain program's by a relative error of at most 0.015.
Values may be sent and summed in bfloat16 or wider, within the bound.
A program may use at most 128 MiB of HBM per device.

v0:
```python
import math

import jax
import jax.numpy as jnp
from jax import lax
from jax.experimental import pallas as pl
from jax.experimental.pallas import tpu as pltpu
from jax.sharding import PartitionSpec as P

D = 2048
HALF = 1024
SEQ = 2
ROWS = 128
TOK = SEQ * ROWS
RCOLS = 384
PCOLS = 256
PAIRS = 3
GROUPS = SEQ * PAIRS
HD = 64
N_SP = 16
COLS = 6 * RCOLS + 2 * PCOLS
OFFS = (0, 384, 768, 1152, 1536, 1920, 2304, 2560)
WIDTHS = (384, 384, 384, 384, 384, 384, 256, 256)
MESH = pl.DeviceIdType.MESH
f32 = jnp.float32
bf16 = jnp.bfloat16


def dot(a, b):
    return lax.dot_general(a, b, (((1,), (0,)), ((), ())), preferred_element_type=f32)


def dot_nt(a, b):
    return lax.dot_general(a, b, (((1,), (1,)), ((), ())), preferred_element_type=f32)


def dot_tn(a, b):
    return lax.dot_general(a, b, (((0,), (0,)), ((), ())), preferred_element_type=f32)


def split2(x):
    hi = x.astype(bf16)
    return hi, (x - hi.astype(f32)).astype(bf16)


def cat(parts, axis):
    return jnp.concatenate(parts, axis=axis)


def sig(x):
    e = jnp.exp(-jnp.abs(x))
    return jnp.where(x >= 0, 1.0, e) / (1.0 + e)


def lane_first(shape):
    return lax.broadcasted_iota(jnp.int32, shape, len(shape) - 1) < HD


def keep(x, head):
    first = lane_first(x.shape)
    zero = jnp.zeros_like(x)
    return jnp.where(first, x, zero) if head == 0 else jnp.where(first, zero, x)


def two_heads(x):
    return cat([keep(x, 0), keep(x, 1)], 0)


def block_ones():
    i = lax.broadcasted_iota(jnp.int32, (128, 128), 0) < HD
    j = lax.broadcasted_iota(jnp.int32, (128, 128), 1) < HD
    return jnp.where(i == j, 1.0, 0.0).astype(bf16)


def head_sums(x, ones2):
    hi, lo = split2(x)
    return dot(cat([hi, lo], 1), ones2)


def prepare(r, k, v, d_in, a_in, d_base, a_base):
    ones = block_ones()
    ones2 = cat([ones, ones], 0)
    x = d_base + d_in
    log_decay = -math.exp(-0.5) * sig(x)
    rate = sig(a_base + a_in)
    unit = k * lax.rsqrt(head_sums(k * k, ones2) + 1.0)
    removal = unit * rate
    i = lax.broadcasted_iota(jnp.int32, (128, 128), 0)
    j = lax.broadcasted_iota(jnp.int32, (128, 128), 1)
    tri = jnp.where(i >= j, 1.0, 0.0).astype(bf16)
    hi, lo = split2(log_decay)
    rest = (log_decay - hi.astype(f32) - lo.astype(f32)).astype(bf16)
    cum = dot(cat([tri, tri], 1), cat([hi, lo], 0)) + dot(tri, rest)
    mid = cum[63:64, :]
    last = cum[127:128, :]
    shrink = jnp.exp(cum - mid)
    grow = jnp.exp(mid - cum)
    alpha = jnp.exp(cum - log_decay - mid) * unit
    rho = r * shrink
    beta = removal * grow
    kappa = k * grow
    return alpha, rho, beta, kappa, jnp.exp(mid), jnp.exp(last - mid), jnp.exp(last)


def pair_products(alpha, rho, beta, kappa):
    x_hi, x_lo = split2(cat([alpha, rho], 0))
    b_hi, b_lo = split2(beta)
    k_hi, k_lo = split2(kappa)
    y_hi = cat([two_heads(b_hi), two_heads(k_hi)], 0)
    y_lo = cat([two_heads(b_lo), two_heads(k_lo)], 0)
    return dot_nt(cat([x_hi, x_lo], 1), cat([y_hi, y_hi], 1)) + dot_nt(x_hi, y_lo)


def block_diag(a, b):
    zero = jnp.zeros_like(a)
    return cat([cat([a, zero], 1), cat([zero, b], 1)], 0)


def masks():
    i = lax.broadcasted_iota(jnp.int32, (128, 256), 0)
    j = lax.broadcasted_iota(jnp.int32, (128, 256), 1) & 127
    return i, j


def inverses(lowers):
    i, j = masks()
    apart = i ^ j
    eye = jnp.where(i == j, 1.0, 0.0)
    inv = [eye - jnp.where(apart == 1, low, 0.0) for low in lowers]
    for level in range(1, 7):
        size = 1 << level
        inside = (apart >= size) & (apart < 2 * size)
        inv_b = [x.astype(bf16) for x in inv]
        steps = [jnp.where(inside, low, 0.0).astype(bf16) for low in lowers]
        half = [
            dot(x, block_diag(c[:, :128], c[:, 128:])).astype(bf16)
            for x, c in zip(inv_b, steps)
        ]
        full = [dot(h, block_diag(x[:, :128], x[:, 128:])) for h, x in zip(half, inv_b)]
        inv = [x - y for x, y in zip(inv, full)]
    return [x.astype(bf16) for x in inv]


def stacked(left, right):
    return cat([cat([keep(left, h), keep(right, h)], 1) for h in (0, 1)], 0)


def solve(inv, low, carried, alpha_full):
    first = dot(inv, stacked(alpha_full.astype(bf16), carried.astype(bf16)))
    first_b = first.astype(bf16)
    l_hi, l_lo = split2(low)
    weights = stacked(first_b[:, :128], first_b[:, 128:])
    back = dot(l_hi, weights) + dot(l_lo, weights)
    kept = first_b.astype(f32)
    miss = (cat([alpha_full, carried], 1) - kept - back).astype(bf16)
    return kept + dot(inv, stacked(miss[:, :128], miss[:, 128:]))


def maps_of(z, value, beta_end, kappa_end, gain_end):
    z_hi, z_lo = split2(z)
    zero = jnp.zeros((128, 128), bf16)
    v_side = cat([zero, -value], 1)
    e_hi, e_lo = split2(cat([beta_end, kappa_end], 0))
    lhs = cat([z_hi, v_side], 0)
    both = dot_tn(lhs, e_hi) + dot_tn(lhs, e_lo) + dot_tn(z_lo, e_hi[:128])
    first = lane_first((64, 128))
    packed = [
        jnp.where(first, both[o : o + 64], both[o + 64 : o + 128]) for o in (0, 128)
    ]
    i = lax.broadcasted_iota(jnp.int32, (64, 128), 0)
    j = lax.broadcasted_iota(jnp.int32, (64, 128), 1) & 63
    transit = jnp.where(i == j, gain_end, 0.0) - packed[0]
    return transit.astype(bf16), (-packed[1]).astype(bf16)


def reads_of(within_beta, z, rho_full, within_value):
    w_hi, w_lo = split2(within_beta)
    z_hi, z_lo = split2(z)
    weights = stacked(z_hi[:, :128], z_hi[:, 128:])
    drop = dot(w_hi, weights) + dot(w_lo, weights)
    drop = drop + dot(w_hi, stacked(z_lo[:, :128], z_lo[:, 128:]))
    return rho_full - drop[:, :128], within_value - drop[:, 128:]


def advance(state, transit, written):
    hi, lo = split2(state)
    moved = dot(cat([hi, lo], 0), two_heads(transit))
    return moved[:64] + moved[64:] + written.astype(f32)


def recurrent_of(reads, state, local):
    hi, lo = split2(reads)
    weights = two_heads(state)
    return dot_nt(cat([hi, lo], 1), cat([weights, weights], 1)) + local


def head_norm(rec, gain, gate):
    ones = block_ones()
    ones2 = cat([ones, ones], 0)
    centred = rec - head_sums(rec, ones2) * (1.0 / HD)
    spread = head_sums(centred * centred, ones2) * (1.0 / HD)
    return (centred * lax.rsqrt(spread + 1.0) * gain * gate * sig(gate)).astype(bf16)


def kernel(
    tok, gain, wr, wk, wv, wd, wa, wg, wp, wgp, dbase, rbase, hgain, mix, pscale, wor, wop, init,
    out,
    tok_v, gain_v, weight_v, acc_v, proj_v, norm_v, base_v, mix_v, pscale_v, wout_v, init_v,
    pool_v, alpha_v, low_v, within_v, rho_v, wval_v, z_v, reads_v, local_v, map_v, maps_in,
    state_v, states_in, merged_v, recout_v, part_v, part_in, out_v,
    w_sem, small_sem, tok_send, tok_recv, halo_send, halo_recv, map_send, map_recv,
    st_send, st_recv, part_send, part_recv, out_sem,
):
    sp = lax.axis_index("sp")
    tp = lax.axis_index("tp")
    other = 1 - tp
    weights = (wr, wk, wv, wd, wa, wg, wp, wgp)
    group_of = lax.div(sp, 2)
    is_owner = (lax.rem(sp, 2) == tp) & (sp < 2 * GROUPS)

    barrier = pltpu.get_barrier_semaphore()
    pl.semaphore_signal(barrier, inc=1, device_id={"tp": other}, device_id_type=MESH)

    @pl.loop(1, N_SP)
    def _(step):
        pl.semaphore_signal(
            barrier, inc=1, device_id={"sp": lax.rem(sp + step, N_SP)}, device_id_type=MESH
        )

    mine = pl.multiple_of(tp * HALF, HALF)
    theirs = pl.multiple_of(other * HALF, HALF)
    rec_at = pl.multiple_of(tp * RCOLS, 128)
    pool_at = pl.multiple_of(tp * PCOLS, 128)
    small = [
        pltpu.make_async_copy(tok, tok_v.at[0], small_sem.at[0]),
        pltpu.make_async_copy(gain.at[:, pl.ds(mine, HALF)], gain_v.at[0], small_sem.at[1]),
        pltpu.make_async_copy(gain.at[:, pl.ds(theirs, HALF)], gain_v.at[1], small_sem.at[2]),
        pltpu.make_async_copy(dbase.at[:, pl.ds(rec_at, RCOLS)], base_v.at[0], small_sem.at[3]),
        pltpu.make_async_copy(rbase.at[:, pl.ds(rec_at, RCOLS)], base_v.at[1], small_sem.at[4]),
        pltpu.make_async_copy(hgain.at[:, pl.ds(rec_at, RCOLS)], base_v.at[2], small_sem.at[5]),
        pltpu.make_async_copy(mix.at[pl.ds(tp * 2, 2)], mix_v, small_sem.at[6]),
        pltpu.make_async_copy(pscale.at[:, pl.ds(pool_at, PCOLS)], pscale_v, small_sem.at[7]),
        pltpu.make_async_copy(init, init_v, small_sem.at[8]),
        pltpu.make_async_copy(wor, wout_v.at[pl.ds(0, RCOLS)], small_sem.at[9]),
        pltpu.make_async_copy(wop, wout_v.at[pl.ds(RCOLS, PCOLS)], small_sem.at[10]),
    ]
    loads = [
        [
            pltpu.make_async_copy(
                w.at[pl.ds(at, HALF)],
                weight_v.at[half, :, pl.ds(OFFS[i], WIDTHS[i])],
                w_sem.at[half, i],
            )
            for i, w in enumerate(weights)
        ]
        for half, at in ((0, mine), (1, theirs))
    ]
    for copy in small[:3]:
        copy.start()
    for half in loads:
        for copy in half:
            copy.start()
    for copy in small[3:]:
        copy.start()

    def take(half):
        wide = tok_v[half].reshape(TOK, HALF).astype(f32)
        norm_v[half] = (wide * gain_v[half]).astype(bf16)
        return jnp.sum(wide * wide, axis=1, keepdims=True)

    for copy in small[:2]:
        copy.wait()
    squares = take(0)

    def tiles_of(step):
        return (3 * step, 3 if step < 3 else 2)

    for step in range(4):
        for copy in loads[0][2 * step : 2 * step + 2]:
            copy.wait()
        start, count = tiles_of(step)

        @pl.loop(start, start + count)
        def _(tile):
            at = pl.ds(pl.multiple_of(tile * 256, 256), 256)
            acc_v[:, at] = dot(norm_v[0], weight_v[0, :, at])

        if step == 1:
            pl.semaphore_wait(barrier, N_SP)
            send_tok = pltpu.make_async_remote_copy(
                src_ref=tok_v.at[0],
                dst_ref=tok_v.at[1],
                send_sem=tok_send,
                recv_sem=tok_recv,
                device_id={"tp": other},
                device_id_type=MESH,
            )
            send_tok.start()

    send_tok.wait_recv()
    small[2].wait()
    squares = squares + take(1)
    scale = lax.rsqrt(squares * (1.0 / D) + 0.25)
    for step in range(4):
        for copy in loads[1][2 * step : 2 * step + 2]:
            copy.wait()
        start, count = tiles_of(step)

        @pl.loop(start, start + count)
        def _(tile):
            at = pl.ds(pl.multiple_of(tile * 256, 256), 256)
            total = acc_v[:, at] + dot(norm_v[1], weight_v[1, :, at])
            proj_v[:, at] = (total * scale).astype(bf16)

    for b in range(SEQ):
        pool_v[b, 16:, :] = proj_v[b * ROWS : (b + 1) * ROWS, OFFS[6] : OFFS[7]]
    halo = pltpu.make_async_remote_copy(
        src_ref=pool_v.at[:, pl.ds(ROWS, 16), :],
        dst_ref=pool_v.at[:, pl.ds(0, 16), :],
        send_sem=halo_send,
        recv_sem=halo_recv,
        device_id={"sp": lax.rem(sp + 1, N_SP)},
        device_id_type=MESH,
    )

    @pl.when(sp < N_SP - 1)
    def _():
        halo.start()

    @pl.when(sp == 0)
    def _():
        pool_v[:, 0:16, :] = jnp.zeros((SEQ, 16, PCOLS), bf16)

    for copy in small[3:6]:
        copy.wait()
    groups = [(b, p) for b in range(SEQ) for p in range(PAIRS)]

    def part(index, b, p):
        at = OFFS[index] + 128 * p
        return proj_v[b * ROWS : (b + 1) * ROWS, at : at + 128]

    i2, j2 = masks()
    strict = i2 > j2
    inclusive = i2 >= j2
    lowers, ends = [], []
    for g, (b, p) in enumerate(groups):
        lanes = pl.ds(128 * p, 128)
        alpha, rho, beta, kappa, e_mid, e_tail, e_last = prepare(
            part(0, b, p).astype(f32),
            part(1, b, p).astype(f32),
            None,
            part(3, b, p).astype(f32),
            part(4, b, p).astype(f32),
            base_v[0, :, lanes],
            base_v[1, :, lanes],
        )
        pairs = pair_products(alpha, rho, beta, kappa)
        low = jnp.where(strict, pairs[:128, :256], 0.0)
        cross = cat(
            [
                jnp.where(strict, pairs[:128, 256:], 0.0),
                jnp.where(inclusive, pairs[128:, 256:], 0.0),
            ],
            0,
        )
        value = part(2, b, p)
        c_hi, c_lo = split2(cross)
        v2 = two_heads(value)
        mixed = dot(c_hi, v2) + dot(c_lo, v2)
        low_v[g] = low
        within_v[g] = jnp.where(inclusive, pairs[128:, :256], 0.0)
        alpha_v[g, 0] = alpha * e_mid
        alpha_v[g, 1] = mixed[:128]
        rho_v[g] = rho * e_mid
        wval_v[g] = mixed[128:]
        ends.append((beta * e_tail, kappa * e_tail, e_last))
    invs = inverses([low_v[g] for g in range(GROUPS)])
    for g, (b, p) in enumerate(groups):
        z = solve(invs[g], low_v[g], alpha_v[g, 1], alpha_v[g, 0])
        z_v[g] = z
        transit, written = maps_of(z, part(2, b, p), *ends[g])
        map_v[g, 0] = transit
        map_v[g, 1] = written

    map_copies = []
    for g in range(GROUPS):
        owner = 2 * g + tp
        copy = pltpu.make_async_remote_copy(
            src_ref=map_v.at[g],
            dst_ref=maps_in.at[sp],
            send_sem=map_send.at[g],
            recv_sem=map_recv.at[sp],
            device_id={"sp": owner},
            device_id_type=MESH,
        )
        map_copies.append(copy)

        @pl.when((sp != owner) & (sp < N_SP - 1))
        def _():
            copy.start()

        @pl.when(sp == owner)
        def _():
            maps_in[sp] = map_v[g]

    for copy in small[6:]:
        copy.wait()

    @pl.when(sp > 0)
    def _():
        halo.wait_recv()

    places = (sp * ROWS + 1 + lax.broadcasted_iota(jnp.int32, (ROWS, 128), 0)).astype(f32)
    for b in range(SEQ):
        outs = []
        for s in range(2):
            at = slice(128 * s, 128 * s + 128)
            own = pool_v[b, :, at].astype(f32)
            total = own + pltpu.roll(own, 1, 0)
            if s == 1:
                total = total + pltpu.roll(total, 2, 0)
            wide = total + pltpu.roll(total, 2 if s == 0 else 4, 0)
            wide = wide + pltpu.roll(wide, 4 if s == 0 else 8, 0)
            trail = jnp.where(tp == 0, total, wide)[16:]
            window = jnp.where(tp == 0, float(2 << s), float(8 << s))
            diff = (trail / jnp.minimum(places, window) - own[16:]).astype(bf16)
            pooled = dot(diff, mix_v[s])
            gate = proj_v[b * ROWS : (b + 1) * ROWS, OFFS[7] + 128 * s : OFFS[7] + 128 * s + 128]
            gate = gate.astype(f32)
            outs.append((pooled * pscale_v[:, at] * (gate * sig(gate))).astype(bf16))
        recout_v[b * ROWS : (b + 1) * ROWS, RCOLS:] = cat(outs, 1)

    @pl.loop(0, 8)
    def _(tile):
        at = pl.ds(pl.multiple_of(tile * 256, 256), 256)
        merged_v[:, at] = dot(recout_v[:, RCOLS:], wout_v[RCOLS:, at])

    def send_state(j):
        return pltpu.make_async_remote_copy(
            src_ref=state_v.at[j],
            dst_ref=states_in.at[group_of],
            send_sem=st_send.at[j],
            recv_sem=st_recv.at[group_of],
            device_id={"sp": j},
            device_id_type=MESH,
        )

    def wait_map(j):
        pltpu.make_async_remote_copy(
            src_ref=map_v.at[0],
            dst_ref=maps_in.at[j],
            send_sem=map_send.at[0],
            recv_sem=map_recv.at[j],
            device_id={"sp": j},
            device_id_type=MESH,
        ).wait_recv()

    @pl.when(is_owner)
    def _():
        seq = lax.div(group_of, PAIRS)
        pair = lax.rem(group_of, PAIRS)
        state0 = cat([init_v[seq, 2 * pair], init_v[seq, 2 * pair + 1]], 1)

        def emit(j, state):
            state_v[j] = state.astype(bf16)

            @pl.when(j != sp)
            def _():
                send_state(j).start()

            @pl.when(j == sp)
            def _():
                states_in[group_of] = state.astype(bf16)

        def body(j, state):
            emit(j, state)

            @pl.when(j != sp)
            def _():
                wait_map(j)

            return advance(state, maps_in[j, 0], maps_in[j, 1])

        emit(N_SP - 1, lax.fori_loop(0, N_SP - 1, body, state0))

    for g in range(GROUPS):
        reads, local = reads_of(
            within_v[g], z_v[g], rho_v[g], wval_v[g]
        )
        reads_v[g] = reads
        local_v[g] = local

    for g, (b, p) in enumerate(groups):
        owner = 2 * g + tp

        @pl.when(sp != owner)
        def _():
            pltpu.make_async_remote_copy(
                src_ref=state_v.at[0],
                dst_ref=states_in.at[g],
                send_sem=st_send.at[0],
                recv_sem=st_recv.at[g],
                device_id={"sp": owner},
                device_id_type=MESH,
            ).wait_recv()

        rec = recurrent_of(reads_v[g], states_in[g], local_v[g])
        lanes = pl.ds(128 * p, 128)
        recout_v[b * ROWS : (b + 1) * ROWS, 128 * p : 128 * p + 128] = head_norm(
            rec, base_v[2, :, lanes], part(5, b, p).astype(f32)
        )

    def product(at):
        return (merged_v[:, at] + dot(recout_v[:, :RCOLS], wout_v[:RCOLS, at])).astype(bf16)

    def send_part(tile):
        return pltpu.make_async_remote_copy(
            src_ref=part_v.at[tile],
            dst_ref=part_in.at[tile],
            send_sem=part_send.at[tile],
            recv_sem=part_recv.at[tile],
            device_id={"tp": other},
            device_id_type=MESH,
        )

    def store_out(tile):
        at = pl.ds(pl.multiple_of(tile * 256, 256), 256)
        return pltpu.make_async_copy(out_v.at[:, :, at], out.at[:, :, at], out_sem.at[tile])

    @pl.loop(0, 4)
    def _(tile):
        at = pl.ds(pl.multiple_of(theirs + tile * 256, 256), 256)
        part_v[tile] = product(at)
        send_part(tile).start()

    @pl.loop(0, 4)
    def _(tile):
        at = pl.ds(pl.multiple_of(mine + tile * 256, 256), 256)
        own = product(at).astype(f32)
        send_part(tile).wait_recv()
        total = (own + part_in[tile].astype(f32)).astype(bf16)
        out_v[:, :, pl.ds(pl.multiple_of(tile * 256, 256), 256)] = total.reshape(SEQ, ROWS, 256)
        store_out(tile).start()

    send_tok.wait_send()

    @pl.when(sp < N_SP - 1)
    def _():
        halo.wait_send()

    for g, copy in enumerate(map_copies):
        @pl.when((sp != 2 * g + tp) & (sp < N_SP - 1))
        def _():
            copy.wait_send()

    @pl.when(is_owner)
    def _():
        @pl.loop(0, N_SP)
        def _(j):
            @pl.when(j != sp)
            def _():
                send_state(j).wait_send()

    @pl.loop(0, 4)
    def _(tile):
        send_part(tile).wait_send()
        store_out(tile).wait()


def shards(
    tokens, norm_gain, w_recept, w_key, w_value, w_decay, w_rate, w_gate_rec, w_pool, w_gate_pool,
    decay_base, rate_base, head_gain, pool_mix, pool_scale, w_out_rec, w_out_pool, init_state,
):
    vmem, sem = pltpu.VMEM, pltpu.SemaphoreType.DMA
    row = lambda x: x.reshape(1, -1)
    scratch = [
        vmem((2, SEQ, ROWS, HALF), bf16),
        vmem((2, 1, HALF), f32),
        vmem((2, HALF, COLS), bf16),
        vmem((TOK, COLS), f32),
        vmem((TOK, COLS), bf16),
        vmem((2, TOK, HALF), bf16),
        vmem((3, 1, RCOLS), f32),
        vmem((2, 128, 128), bf16),
        vmem((1, PCOLS), f32),
        vmem((RCOLS + PCOLS, D), bf16),
        vmem((SEQ, 2 * PAIRS, HD, HD), f32),
        vmem((SEQ, 16 + ROWS, PCOLS), bf16),
        vmem((GROUPS, 2, 128, 128), f32),
        vmem((GROUPS, 128, 256), f32),
        vmem((GROUPS, 128, 256), f32),
        vmem((GROUPS, 128, 128), f32),
        vmem((GROUPS, 128, 128), f32),
        vmem((GROUPS, 128, 256), f32),
        vmem((GROUPS, 128, 128), f32),
        vmem((GROUPS, 128, 128), f32),
        vmem((GROUPS, 2, HD, 128), bf16),
        vmem((N_SP, 2, HD, 128), bf16),
        vmem((N_SP, HD, 128), bf16),
        vmem((GROUPS, HD, 128), bf16),
        vmem((TOK, D), f32),
        vmem((TOK, RCOLS + PCOLS), bf16),
        vmem((4, TOK, 256), bf16),
        vmem((4, TOK, 256), bf16),
        vmem((SEQ, ROWS, HALF), bf16),
        sem((2, 8)),
        sem((11,)),
        sem,
        sem,
        sem,
        sem,
        sem((GROUPS,)),
        sem((N_SP,)),
        sem((N_SP,)),
        sem((GROUPS,)),
        sem((4,)),
        sem((4,)),
        sem((4,)),
    ]
    return pl.pallas_call(
        kernel,
        out_shape=jax.ShapeDtypeStruct((SEQ, ROWS, HALF), bf16),
        in_specs=[pl.BlockSpec(memory_space=pl.ANY)] * 18,
        out_specs=pl.BlockSpec(memory_space=pl.ANY),
        scratch_shapes=scratch,
        compiler_params=pltpu.CompilerParams(
            collective_id=0, has_side_effects=True, vmem_limit_bytes=56 << 20
        ),
        name="layer",
    )(
        tokens, row(norm_gain), w_recept, w_key, w_value, w_decay, w_rate, w_gate_rec, w_pool,
        w_gate_pool, row(decay_base), row(rate_base), row(head_gain), pool_mix, row(pool_scale),
        w_out_rec, w_out_pool, init_state,
    )


def solution(mesh):
    split = P(None, "tp")
    placed = (
        P("fs", "sp", "tp"), P(),
        split, split, split, split, split, split, split, split,
        P(), P(), P(), P(), P(),
        P("tp", None), P("tp", None), P("fs", "tp", None, None),
    )
    return jax.shard_map(
        shards, mesh=mesh, in_specs=placed, out_specs=P("fs", "sp", "tp"), check_vma=False
    )
```

profile of v0, /device:TPU:1, one launch (start us, length us, event | category | flops | bytes accessed | tf_op | source)
XLA Modules:
  0.0 42.1 jit_solution(4399411825406383958)
XLA Ops:
  0.0 1.3 %reshape.16.dbase = f32[1,768]{1,0:T(1,128)} reshape(f32[768]{0:T(1024)} %param.28) | data formatting | bytes 6144 | tf_op jit(solution)/shard_map/reshape | solution.py:575
  1.3 1.3 %reshape.17.rbase = f32[1,768]{1,0:T(1,128)} reshape(f32[768]{0:T(1024)} %param.29) | data formatting | bytes 6144 | tf_op jit(solution)/shard_map/reshape | solution.py:575
  2.5 1.3 %reshape.18.hgain = f32[1,768]{1,0:T(1,128)} reshape(f32[768]{0:T(1024)} %param.30) | data formatting | bytes 6144 | tf_op jit(solution)/shard_map/reshape | solution.py:575
  3.8 36.4 %layer.1 = bf16[2,128,1024]{2,1,0:T(8,128)(2,1)} custom-call(bf16[2,128,1024]{2,1,0:T(8,128)(2,1)} %tok.1, f32[1,2048]{1,0:T(1,128)} %bitcast.2, bf16[2048,384]{1,0:T(8,128)(2,1)} %wr.1, bf16[2048,384]{1,0:T(8,128)(2,1)} %wk.1, bf16[2048,384]{1,0:T(8,128)(2,1)} %wv.1, bf16[2048,384]{1,0:T(8,128)(2,1)} %wd.1, bf16[2048,384]{1,0:T(8,128)(2,1)} %wa.1, ...), custom_call_target="tpu_custom_call" | custom-call | tf_op jit(solution)/shard_map/layer/pallas_call | solution.py:620
  40.2 1.9 %copy.20 = bf16[2,128,1024]{2,1,0:T(8,128)(2,1)} copy(bf16[2,128,1024]{2,1,0:T(8,128)(2,1)} %layer.1) | data formatting | bytes 1048576
where the time goes:
time: 42.3 us; the launch traced here: 42.1 us
  Pallas kernels  36.4 us (86%)
  local copies, waits for them, and re-layouts  5.69 us (13%)
    pallas_call x1, Pallas kernels, shards(): pl.pallas_call(kernel, out_shape=jax.ShapeDtypeStruct((SEQ, ROWS, HALF),...  36.4 us
    reshape x3, local copies, waits for them, and re-layouts, shards(): row = lambda x: x.reshape(1, -1)  3.82 us
    unnamed x1, local copies, waits for them, and re-layouts  1.87 us

commit v1 on v0

v1 whole, which is shorter than its diff:
```python
import math

import jax
import jax.numpy as jnp
from jax import lax
from jax.experimental import pallas as pl
from jax.experimental.pallas import tpu as pltpu
from jax.sharding import PartitionSpec as P

D = 2048
HALF = 1024
SEQ = 2
ROWS = 128
TOK = SEQ * ROWS
RCOLS = 384
PCOLS = 256
PAIRS = 3
GROUPS = SEQ * PAIRS
HD = 64
N_SP = 16
COLS = 6 * RCOLS + 2 * PCOLS
OFFS = (0, 384, 768, 1152, 1536, 1920, 2304, 2560)
WIDTHS = (384, 384, 384, 384, 384, 384, 256, 256)
MESH = pl.DeviceIdType.MESH
f32 = jnp.float32
bf16 = jnp.bfloat16


def dot(a, b):
    return lax.dot_general(a, b, (((1,), (0,)), ((), ())), preferred_element_type=f32)


def dot_nt(a, b):
    return lax.dot_general(a, b, (((1,), (1,)), ((), ())), preferred_element_type=f32)


def dot_tn(a, b):
    return lax.dot_general(a, b, (((0,), (0,)), ((), ())), preferred_element_type=f32)


def split2(x):
    hi = x.astype(bf16)
    return hi, (x - hi.astype(f32)).astype(bf16)


def cat(parts, axis):
    return jnp.concatenate(parts, axis=axis)


def sig(x):
    e = jnp.exp(-jnp.abs(x))
    return jnp.where(x >= 0, 1.0, e) / (1.0 + e)


def lane_first(shape):
    return lax.broadcasted_iota(jnp.int32, shape, len(shape) - 1) < HD


def keep(x, head):
    first = lane_first(x.shape)
    zero = jnp.zeros_like(x)
    return jnp.where(first, x, zero) if head == 0 else jnp.where(first, zero, x)


def two_heads(x):
    return cat([keep(x, 0), keep(x, 1)], 0)


def block_ones():
    i = lax.broadcasted_iota(jnp.int32, (128, 128), 0) < HD
    j = lax.broadcasted_iota(jnp.int32, (128, 128), 1) < HD
    return jnp.where(i == j, 1.0, 0.0).astype(bf16)


def head_sums(x, ones2):
    hi, lo = split2(x)
    return dot(cat([hi, lo], 1), ones2)


def prepare(r, k, d_in, a_in, d_base, a_base):
    ones = block_ones()
    ones2 = cat([ones, ones], 0)
    x = d_base + d_in
    log_decay = -math.exp(-0.5) * sig(x)
    rate = sig(a_base + a_in)
    squares = k * k
    sums = cat([head_sums(squares[:, o : o + 128], ones2) for o in range(0, RCOLS, 128)], 1)
    unit = k * lax.rsqrt(sums + 1.0)
    removal = unit * rate
    i = lax.broadcasted_iota(jnp.int32, (128, 128), 0)
    j = lax.broadcasted_iota(jnp.int32, (128, 128), 1)
    tri = jnp.where(i >= j, 1.0, 0.0).astype(bf16)
    hi, lo = split2(log_decay)
    rest = (log_decay - hi.astype(f32) - lo.astype(f32)).astype(bf16)
    cum = dot(cat([tri, tri, tri], 1), cat([hi, lo, rest], 0))
    mid = cum[63:64, :]
    last = cum[127:128, :]
    shrink = jnp.exp(cum - mid)
    grow = jnp.exp(mid - cum)
    alpha = jnp.exp(cum - log_decay - mid) * unit
    rho = r * shrink
    beta = removal * grow
    kappa = k * grow
    return alpha, rho, beta, kappa, jnp.exp(mid), jnp.exp(last - mid), jnp.exp(last)


def pair_products(x, beta, kappa):
    x_hi, x_lo = split2(x)
    b_hi, b_lo = split2(beta)
    k_hi, k_lo = split2(kappa)
    y_hi = cat([two_heads(b_hi), two_heads(k_hi)], 0)
    y_lo = cat([two_heads(b_lo), two_heads(k_lo)], 0)
    return dot_nt(cat([x_hi, x_lo], 1), cat([y_hi, y_hi], 1)) + dot_nt(x_hi, y_lo)


def block_diag(x):
    a, b = x[:, :128], x[:, 128:]
    zero = jnp.zeros_like(a)
    return cat([cat([a, zero], 1), cat([zero, b], 1)], 0)


def masks():
    i = lax.broadcasted_iota(jnp.int32, (128, 256), 0)
    j = lax.broadcasted_iota(jnp.int32, (128, 256), 1) & 127
    return i, j


def inverses(lowers):
    i, j = masks()
    apart = i ^ j
    eye = jnp.where(i == j, 1.0, 0.0)
    zero = jnp.zeros((128, 256), bf16)
    inv = [eye - jnp.where(apart == 1, low, zero).astype(f32) for low in lowers]
    for size in (2, 8, 32):
        inside = (apart >= size) & (apart < 4 * size)
        inv_b = [block_diag(x.astype(bf16)) for x in inv]
        steps = [block_diag(jnp.where(inside, low, zero)) for low in lowers]
        hop = [dot(x.astype(bf16), c).astype(bf16) for x, c in zip(inv, steps)]
        twice = [dot(h, block_diag(h)).astype(bf16) for h in hop]
        once = [x - dot(h, b) for x, h, b in zip(inv, hop, inv_b)]
        inv = [x + dot(t, block_diag(x.astype(bf16))) for x, t in zip(once, twice)]
    return [x.astype(bf16) for x in inv]


def stacked(x):
    left, right = x[:, :128], x[:, 128:]
    return cat([cat([keep(left, h), keep(right, h)], 1) for h in (0, 1)], 0)


def solve_all(invs, lows, sides):
    first = [dot(inv, stacked(side.astype(bf16))).astype(bf16) for inv, side in zip(invs, sides)]
    back = [dot(low, stacked(x)) for low, x in zip(lows, first)]
    miss = [
        (side - x.astype(f32) - y).astype(bf16) for side, x, y in zip(sides, first, back)
    ]
    return [x.astype(f32) + dot(inv, stacked(m)) for x, inv, m in zip(first, invs, miss)]


def maps_of(z, value, beta_end, kappa_end, gain_end):
    zero = jnp.zeros((128, 128), bf16)
    lhs = cat([z.astype(bf16), cat([zero, -value], 1)], 0)
    both = dot_tn(lhs, cat([beta_end, kappa_end], 0).astype(bf16))
    first = lane_first((64, 128))
    packed = [
        jnp.where(first, both[o : o + 64], both[o + 64 : o + 128]) for o in (0, 128)
    ]
    i = lax.broadcasted_iota(jnp.int32, (64, 128), 0)
    j = lax.broadcasted_iota(jnp.int32, (64, 128), 1) & 63
    transit = jnp.where(i == j, gain_end, 0.0) - packed[0]
    return transit.astype(bf16), (-packed[1]).astype(bf16)


def after(left, transit, written):
    l_hi, l_lo = split2(left)
    t_hi, t_lo = split2(transit)
    weights = two_heads(t_hi)
    moved = dot(cat([l_hi, l_lo], 1), cat([weights, weights], 0)) + dot(l_hi, two_heads(t_lo))
    return moved + written


def after_given(left, transit):
    hi, lo = split2(left)
    weights = two_heads(transit)
    return dot(cat([hi, lo], 1), cat([weights, weights], 0))


def recurrent_of(reads, state, local):
    hi, lo = split2(reads)
    weights = two_heads(state)
    return dot_nt(cat([hi, lo], 1), cat([weights, weights], 1)) + local


def head_norm(rec, gain, gate):
    ones = block_ones()
    ones2 = cat([ones, ones], 0)
    offs = range(0, RCOLS, 128)
    total = cat([head_sums(rec[:, o : o + 128], ones2) for o in offs], 1)
    centred = rec - total * (1.0 / HD)
    squares = centred * centred
    spread = cat([head_sums(squares[:, o : o + 128], ones2) for o in offs], 1) * (1.0 / HD)
    return (centred * lax.rsqrt(spread + 1.0) * gain * gate * sig(gate)).astype(bf16)


def kernel(
    tok, gain, wr, wk, wv, wd, wa, wg, wp, wgp, dbase, rbase, hgain, mix, pscale, wor, wop, init,
    out,
    tok_v, gain_v, weight_v, acc_v, proj_v, norm_v, base_v, mix_v, pscale_v, wout_v, init_v,
    pool_v, keys_v, low_v, side_v, z_v, reads_v, local_v, map_v, maps_in,
    state_v, states_in, merged_v, recout_v, part_v, part_in, part_own, out_v,
    w_sem, small_sem, tok_send, tok_recv, halo_send, halo_recv, map_send, map_recv,
    st_send, st_recv, part_send, part_recv, out_sem,
):
    sp = lax.axis_index("sp")
    tp = lax.axis_index("tp")
    other = 1 - tp
    weights = (wr, wk, wv, wd, wa, wg, wp, wgp)
    group_of = lax.div(sp, 2)
    is_owner = (lax.rem(sp, 2) == tp) & (sp < 2 * GROUPS)

    barrier = pltpu.get_barrier_semaphore()
    pl.semaphore_signal(barrier, inc=1, device_id={"tp": other}, device_id_type=MESH)

    @pl.loop(1, N_SP)
    def _(step):
        pl.semaphore_signal(
            barrier, inc=1, device_id={"sp": lax.rem(sp + step, N_SP)}, device_id_type=MESH
        )

    mine = pl.multiple_of(tp * HALF, HALF)
    theirs = pl.multiple_of(other * HALF, HALF)
    pool_at = pl.multiple_of(tp * PCOLS, 128)
    small = [
        pltpu.make_async_copy(tok, tok_v.at[0], small_sem.at[0]),
        pltpu.make_async_copy(gain.at[:, pl.ds(mine, HALF)], gain_v.at[0], small_sem.at[1]),
        pltpu.make_async_copy(gain.at[:, pl.ds(theirs, HALF)], gain_v.at[1], small_sem.at[2]),
        pltpu.make_async_copy(dbase, base_v.at[0], small_sem.at[3]),
        pltpu.make_async_copy(rbase, base_v.at[1], small_sem.at[4]),
        pltpu.make_async_copy(hgain, base_v.at[2], small_sem.at[5]),
        pltpu.make_async_copy(mix.at[pl.ds(tp * 2, 2)], mix_v, small_sem.at[6]),
        pltpu.make_async_copy(pscale.at[:, pl.ds(pool_at, PCOLS)], pscale_v, small_sem.at[7]),
        pltpu.make_async_copy(init, init_v, small_sem.at[8]),
        pltpu.make_async_copy(wor, wout_v.at[pl.ds(0, RCOLS)], small_sem.at[9]),
        pltpu.make_async_copy(wop, wout_v.at[pl.ds(RCOLS, PCOLS)], small_sem.at[10]),
    ]
    loads = [
        [
            pltpu.make_async_copy(
                w.at[pl.ds(at, HALF)],
                weight_v.at[half, :, pl.ds(OFFS[i], WIDTHS[i])],
                w_sem.at[half, i],
            )
            for i, w in enumerate(weights)
        ]
        for half, at in ((0, mine), (1, theirs))
    ]
    def start(copies):
        for copy in copies:
            copy.start()

    start(small[:3])
    start(loads[0][:4])

    def take(half):
        wide = tok_v[half].reshape(TOK, HALF).astype(f32)
        norm_v[half] = (wide * gain_v[half]).astype(bf16)
        return jnp.sum(wide * wide, axis=1, keepdims=True)

    for copy in small[:2]:
        copy.wait()
    start(loads[0][4:] + loads[1][:2])
    squares = take(0)

    def columns(step):
        return slice(768 * step, min(768 * step + 768, COLS))

    for step in range(4):
        for copy in loads[0][2 * step : 2 * step + 2]:
            copy.wait()
        at = columns(step)
        acc_v[:, at] = dot(norm_v[0], weight_v[0, :, at])
        start((loads[1][2:4], loads[1][4:], small[3:], [])[step])
        if step == 0:
            pl.semaphore_wait(barrier, N_SP)
            send_tok = pltpu.make_async_remote_copy(
                src_ref=tok_v.at[0],
                dst_ref=tok_v.at[1],
                send_sem=tok_send,
                recv_sem=tok_recv,
                device_id={"tp": other},
                device_id_type=MESH,
            )
            send_tok.start()

    send_tok.wait_recv()
    small[2].wait()
    squares = squares + take(1)
    scale = lax.rsqrt(squares * (1.0 / D) + 0.25)
    for step in range(4):
        for copy in loads[1][2 * step : 2 * step + 2]:
            copy.wait()
        at = columns(step)
        total = acc_v[:, at] + dot(norm_v[1], weight_v[1, :, at])
        proj_v[:, at] = (total * scale).astype(bf16)

    for b in range(SEQ):
        pool_v[b, 16:, :] = proj_v[b * ROWS : (b + 1) * ROWS, OFFS[6] : OFFS[7]]
    halo = pltpu.make_async_remote_copy(
        src_ref=pool_v.at[:, pl.ds(ROWS, 16), :],
        dst_ref=pool_v.at[:, pl.ds(0, 16), :],
        send_sem=halo_send,
        recv_sem=halo_recv,
        device_id={"sp": lax.rem(sp + 1, N_SP)},
        device_id_type=MESH,
    )

    @pl.when(sp < N_SP - 1)
    def _():
        halo.start()

    @pl.when(sp == 0)
    def _():
        pool_v[:, 0:16, :] = jnp.zeros((SEQ, 16, PCOLS), bf16)

    for copy in small[3:6]:
        copy.wait()
    groups = [(b, p) for b in range(SEQ) for p in range(PAIRS)]

    def part(index, b, p):
        at = OFFS[index] + 128 * p
        return proj_v[b * ROWS : (b + 1) * ROWS, at : at + 128]

    i2, j2 = masks()
    strict = i2 > j2
    inclusive = i2 >= j2

    def rows_of(index, b):
        at = OFFS[index]
        return proj_v[b * ROWS : (b + 1) * ROWS, at : at + WIDTHS[index]].astype(f32)

    def local_row(index):
        return cat([base_v[index, pl.ds(3 * tp + p, 1), :] for p in range(PAIRS)], 1)

    ends = []
    for b in range(SEQ):
        alpha, rho, beta, kappa, e_mid, e_tail, e_last = prepare(
            rows_of(0, b), rows_of(1, b), rows_of(3, b), rows_of(4, b), local_row(0), local_row(1)
        )
        keys_v[b, 0] = alpha
        keys_v[b, 1] = rho
        keys_v[b, 2] = beta
        keys_v[b, 3] = kappa
        ends.append((e_mid, e_tail, e_last))

    def pair_of(index, g):
        b, p = groups[g]
        return keys_v[b, index, :, 128 * p : 128 * p + 128]

    def end_of(index, g):
        b, p = groups[g]
        return ends[b][index][:, 128 * p : 128 * p + 128]

    every = range(GROUPS)
    for g in every:
        pairs = pair_products(pair_of(0, g), pair_of(2, g), pair_of(3, g))
        low_v[g] = jnp.where(strict, pairs[:, :256], 0.0).astype(bf16)
        cross = jnp.where(strict, pairs[:, 256:], 0.0).astype(bf16)
        side_v[g, :, :128] = pair_of(0, g) * end_of(0, g)
        side_v[g, :, 128:] = dot(cross, two_heads(part(2, *groups[g])))
    invs = inverses([low_v[g] for g in every])
    map_copies = []
    for some in (range(0, 3), range(3, 6)):
        solved = solve_all(
            [invs[g] for g in some], [low_v[g] for g in some], [side_v[g] for g in some]
        )
        for g, z in zip(some, solved):
            z_v[g] = z.astype(bf16)
            tail = end_of(1, g)
            transit, written = maps_of(
                z, part(2, *groups[g]), pair_of(2, g) * tail, pair_of(3, g) * tail, end_of(2, g)
            )
            map_v[g, 0] = transit
            map_v[g, 1] = written
        for g in some:
            owner = 2 * g + tp
            copy = pltpu.make_async_remote_copy(
                src_ref=map_v.at[g],
                dst_ref=maps_in.at[sp],
                send_sem=map_send.at[g],
                recv_sem=map_recv.at[sp],
                device_id={"sp": owner},
                device_id_type=MESH,
            )
            map_copies.append(copy)

            @pl.when((sp != owner) & (sp < N_SP - 1))
            def _():
                copy.start()

            @pl.when(sp == owner)
            def _():
                pltpu.make_async_copy(map_v.at[g], maps_in.at[sp], map_recv.at[sp]).start()

    for copy in small[6:]:
        copy.wait()

    @pl.when(sp > 0)
    def _():
        halo.wait_recv()

    places = (sp * ROWS + 1 + lax.broadcasted_iota(jnp.int32, (ROWS, 128), 0)).astype(f32)
    for b in range(SEQ):
        outs = []
        for s in range(2):
            at = slice(128 * s, 128 * s + 128)
            own = pool_v[b, :, at].astype(f32)
            total = own + pltpu.roll(own, 1, 0)
            if s == 1:
                total = total + pltpu.roll(total, 2, 0)
            wide = total + pltpu.roll(total, 2 if s == 0 else 4, 0)
            wide = wide + pltpu.roll(wide, 4 if s == 0 else 8, 0)
            trail = jnp.where(tp == 0, total, wide)[16:]
            window = jnp.where(tp == 0, float(2 << s), float(8 << s))
            diff = (trail / jnp.minimum(places, window) - own[16:]).astype(bf16)
            pooled = dot(diff, mix_v[s])
            gate = proj_v[b * ROWS : (b + 1) * ROWS, OFFS[7] + 128 * s : OFFS[7] + 128 * s + 128]
            gate = gate.astype(f32)
            outs.append((pooled * pscale_v[:, at] * (gate * sig(gate))).astype(bf16))
        recout_v[b * ROWS : (b + 1) * ROWS, RCOLS:] = cat(outs, 1)

    for at in (slice(0, 1024), slice(1024, D)):
        merged_v[:, at] = dot(recout_v[:, RCOLS:], wout_v[RCOLS:, at])

    def send_state(j):
        return pltpu.make_async_remote_copy(
            src_ref=state_v.at[j],
            dst_ref=states_in.at[group_of],
            send_sem=st_send.at[j],
            recv_sem=st_recv.at[group_of],
            device_id={"sp": j},
            device_id_type=MESH,
        )

    def wait_map(j):
        pltpu.make_async_copy(map_v.at[0], maps_in.at[j], map_recv.at[j]).wait()

    @pl.when(is_owner)
    def _():
        seq = lax.div(group_of, PAIRS)
        pair = lax.rem(group_of, PAIRS)
        state = cat([init_v[seq, 2 * pair], init_v[seq, 2 * pair + 1]], 1)
        for j in range(N_SP - 1):
            wait_map(j)
        zero = jnp.zeros((HD, 128), f32)
        prefixes = []
        for block in range(4):
            held = [cat([maps_in[4 * block, 0], maps_in[4 * block, 1]], 0).astype(f32)]
            prefixes.append(held)
        for y in (1, 2, 3):
            for block in range(4):
                j = 4 * block + y
                if j < N_SP - 1:
                    held = prefixes[block]
                    moved = after_given(held[-1], maps_in[j, 0])
                    held.append(moved + cat([zero, maps_in[j, 1].astype(f32)], 0))
        for block in range(4):
            held = prefixes[block]
            state_v[4 * block] = state.astype(bf16)
            for y in (1, 2, 3):
                inside = held[y - 1]
                state_v[4 * block + y] = after(state, inside[:HD], inside[HD:]).astype(bf16)
            if block < 3:
                state = after(state, held[3][:HD], held[3][HD:])

        @pl.loop(0, N_SP)
        def _(j):
            @pl.when(j != sp)
            def _():
                send_state(j).start()

            @pl.when(j == sp)
            def _():
                pltpu.make_async_copy(
                    state_v.at[j], states_in.at[group_of], st_recv.at[group_of]
                ).start()

    for g in every:
        pairs = pair_products(pair_of(1, g), pair_of(2, g), pair_of(3, g))
        within_beta = jnp.where(inclusive, pairs[:, :256], 0.0).astype(bf16)
        within_kappa = jnp.where(inclusive, pairs[:, 256:], 0.0).astype(bf16)
        drop = dot(within_beta, stacked(z_v[g]))
        reads_v[g] = pair_of(1, g) * end_of(0, g) - drop[:, :128]
        local_v[g] = dot(within_kappa, two_heads(part(2, *groups[g]))) - drop[:, 128:]

    for b in range(SEQ):
        recs = []
        for g in range(PAIRS * b, PAIRS * b + PAIRS):
            pltpu.make_async_copy(state_v.at[0], states_in.at[g], st_recv.at[g]).wait()
            recs.append(recurrent_of(reads_v[g], states_in[g], local_v[g]))
        recout_v[b * ROWS : (b + 1) * ROWS, :RCOLS] = head_norm(
            cat(recs, 1), local_row(2), rows_of(5, b)
        )

    def product(at):
        return (merged_v[:, at] + dot(recout_v[:, :RCOLS], wout_v[:RCOLS, at])).astype(bf16)

    def send_part(tile):
        return pltpu.make_async_remote_copy(
            src_ref=part_v.at[tile],
            dst_ref=part_in.at[tile],
            send_sem=part_send.at[tile],
            recv_sem=part_recv.at[tile],
            device_id={"tp": other},
            device_id_type=MESH,
        )

    def store_out(tile):
        at = pl.ds(512 * tile, 512)
        return pltpu.make_async_copy(out_v.at[:, :, at], out.at[:, :, at], out_sem.at[tile])

    for tile in range(2):
        part_v[tile] = product(pl.ds(pl.multiple_of(theirs + tile * 512, 512), 512))
        send_part(tile).start()
    for tile in range(2):
        part_own[tile] = product(pl.ds(pl.multiple_of(mine + tile * 512, 512), 512))
    for tile in range(2):
        send_part(tile).wait_recv()
        total = part_own[tile].astype(f32) + part_in[tile].astype(f32)
        out_v[:, :, 512 * tile : 512 * tile + 512] = total.astype(bf16).reshape(SEQ, ROWS, 512)
        store_out(tile).start()

    send_tok.wait_send()

    @pl.when(sp < N_SP - 1)
    def _():
        halo.wait_send()

    for g, copy in enumerate(map_copies):
        @pl.when((sp != 2 * g + tp) & (sp < N_SP - 1))
        def _():
            copy.wait_send()

    @pl.when(is_owner)
    def _():
        @pl.loop(0, N_SP)
        def _(j):
            @pl.when(j != sp)
            def _():
                send_state(j).wait_send()

    for tile in range(2):
        send_part(tile).wait_send()
        store_out(tile).wait()


def shards(
    tokens, norm_gain, w_recept, w_key, w_value, w_decay, w_rate, w_gate_rec, w_pool, w_gate_pool,
    decay_base, rate_base, head_gain, pool_mix, pool_scale, w_out_rec, w_out_pool, init_state,
):
    vmem, sem = pltpu.VMEM, pltpu.SemaphoreType.DMA
    row = lambda x: x.reshape(1, -1)
    tile = lambda x: x.reshape(6, 128)
    scratch = [
        vmem((2, SEQ, ROWS, HALF), bf16),
        vmem((2, 1, HALF), f32),
        vmem((2, HALF, COLS), bf16),
        vmem((TOK, COLS), f32),
        vmem((TOK, COLS), bf16),
        vmem((2, TOK, HALF), bf16),
        vmem((3, 6, 128), f32),
        vmem((2, 128, 128), bf16),
        vmem((1, PCOLS), f32),
        vmem((RCOLS + PCOLS, D), bf16),
        vmem((SEQ, 2 * PAIRS, HD, HD), f32),
        vmem((SEQ, 16 + ROWS, PCOLS), bf16),
        vmem((SEQ, 4, ROWS, RCOLS), f32),
        vmem((GROUPS, 128, 256), bf16),
        vmem((GROUPS, 128, 256), f32),
        vmem((GROUPS, 128, 256), bf16),
        vmem((GROUPS, 128, 128), f32),
        vmem((GROUPS, 128, 128), f32),
        vmem((GROUPS, 2, HD, 128), bf16),
        vmem((N_SP, 2, HD, 128), bf16),
        vmem((N_SP, HD, 128), bf16),
        vmem((GROUPS, HD, 128), bf16),
        vmem((TOK, D), f32),
        vmem((TOK, RCOLS + PCOLS), bf16),
        vmem((2, TOK, 512), bf16),
        vmem((2, TOK, 512), bf16),
        vmem((2, TOK, 512), bf16),
        vmem((SEQ, ROWS, HALF), bf16),
        sem((2, 8)),
        sem((11,)),
        sem,
        sem,
        sem,
        sem,
        sem((GROUPS,)),
        sem((N_SP,)),
        sem((N_SP,)),
        sem((GROUPS,)),
        sem((2,)),
        sem((2,)),
        sem((2,)),
    ]
    return pl.pallas_call(
        kernel,
        out_shape=jax.ShapeDtypeStruct((SEQ, ROWS, HALF), bf16),
        in_specs=[pl.BlockSpec(memory_space=pl.ANY)] * 18,
        out_specs=pl.BlockSpec(memory_space=pl.ANY),
        scratch_shapes=scratch,
        compiler_params=pltpu.CompilerParams(
            collective_id=0, has_side_effects=True, vmem_limit_bytes=56 << 20
        ),
        name="layer",
    )(
        tokens, row(norm_gain), w_recept, w_key, w_value, w_decay, w_rate, w_gate_rec, w_pool,
        w_gate_pool, tile(decay_base), tile(rate_base), tile(head_gain), pool_mix, row(pool_scale),
        w_out_rec, w_out_pool, init_state,
    )


def solution(mesh):
    split = P(None, "tp")
    placed = (
        P("fs", "sp", "tp"), P(),
        split, split, split, split, split, split, split, split,
        P(), P(), P(), P(), P(),
        P("tp", None), P("tp", None), P("fs", "tp", None, None),
    )
    return jax.shard_map(
        shards, mesh=mesh, in_specs=placed, out_specs=P("fs", "sp", "tp"), check_vma=False
    )
```

time: 42.3 us -> 36 us (0.85)
  local copies, waits for them, and re-layouts: 5.69 us -> 1.87 us
  Pallas kernels: 36.4 us -> 33.9 us
    reshape x3 -> x0, local copies, waits for them, and re-layouts: 3.82 us -> none  [shards(): row = lambda x: x.reshape(1, -1)]
    pallas_call x1, Pallas kernels: 36.4 us -> 33.9 us  [shards(): pl.pallas_call(kernel, out_shape=jax.ShapeDtypeStruct((SEQ, ROWS, HALF),...]
where the time goes in v1:
time: 36 us; the launch traced here: 35.8 us
  Pallas kernels  33.9 us (94%)
  local copies, waits for them, and re-layouts  1.87 us (5%)
    pallas_call x1, Pallas kernels, shards(): pl.pallas_call(kernel, out_shape=jax.ShapeDtypeStruct((SEQ, ROWS, HALF),...  33.9 us
    unnamed x1, local copies, waits for them, and re-layouts  1.87 us

profile of v1, /device:TPU:1, one launch (start us, length us, event | category | flops | bytes accessed | tf_op | source)
XLA Modules:
  0.0 35.8 jit_solution(3990588066845906730)
XLA Ops:
  0.0 33.9 %layer.1 = bf16[2,128,1024]{2,1,0:T(8,128)(2,1)} custom-call(bf16[2,128,1024]{2,1,0:T(8,128)(2,1)} %tok.1, f32[1,2048]{1,0:T(1,128)} %bitcast.5, bf16[2048,384]{1,0:T(8,128)(2,1)} %wr.1, bf16[2048,384]{1,0:T(8,128)(2,1)} %wk.1, bf16[2048,384]{1,0:T(8,128)(2,1)} %wv.1, bf16[2048,384]{1,0:T(8,128)(2,1)} %wd.1, bf16[2048,384]{1,0:T(8,128)(2,1)} %wa.1, ...), custom_call_target="tpu_custom_call" | custom-call | tf_op jit(solution)/shard_map/layer/pallas_call | solution.py:605
  33.9 1.9 %copy.20 = bf16[2,128,1024]{2,1,0:T(8,128)(2,1)} copy(bf16[2,128,1024]{2,1,0:T(8,128)(2,1)} %layer.1) | data formatting | bytes 1048576

commit v2 on v1

--- a/solution.py
+++ b/solution.py
@@ -19,7 +19,9 @@
 HD = 64
 N_SP = 16
 COLS = 6 * RCOLS + 2 * PCOLS
-OFFS = (0, 384, 768, 1152, 1536, 1920, 2304, 2560)
+OFFS = (1536, 0, 1152, 384, 768, 1920, 2304, 2560)
+NEED = (1, 3, 4, 2, 0, 5, 6, 7)
+EARLY = 4 * RCOLS
 WIDTHS = (384, 384, 384, 384, 384, 384, 256, 256)
 MESH = pl.DeviceIdType.MESH
 f32 = jnp.float32
@@ -77,7 +79,7 @@
     return dot(cat([hi, lo], 1), ones2)
 
 
-def prepare(r, k, d_in, a_in, d_base, a_base):
+def prepare(k, d_in, a_in, d_base, a_base):
     ones = block_ones()
     ones2 = cat([ones, ones], 0)
     x = d_base + d_in
@@ -98,62 +100,48 @@
     shrink = jnp.exp(cum - mid)
     grow = jnp.exp(mid - cum)
     alpha = jnp.exp(cum - log_decay - mid) * unit
-    rho = r * shrink
     beta = removal * grow
     kappa = k * grow
-    return alpha, rho, beta, kappa, jnp.exp(mid), jnp.exp(last - mid), jnp.exp(last)
-
-
-def pair_products(x, beta, kappa):
-    x_hi, x_lo = split2(x)
-    b_hi, b_lo = split2(beta)
-    k_hi, k_lo = split2(kappa)
-    y_hi = cat([two_heads(b_hi), two_heads(k_hi)], 0)
-    y_lo = cat([two_heads(b_lo), two_heads(k_lo)], 0)
-    return dot_nt(cat([x_hi, x_lo], 1), cat([y_hi, y_hi], 1)) + dot_nt(x_hi, y_lo)
-
-
-def block_diag(x):
-    a, b = x[:, :128], x[:, 128:]
-    zero = jnp.zeros_like(a)
-    return cat([cat([a, zero], 1), cat([zero, b], 1)], 0)
-
-
-def masks():
-    i = lax.broadcasted_iota(jnp.int32, (128, 256), 0)
-    j = lax.broadcasted_iota(jnp.int32, (128, 256), 1) & 127
-    return i, j
+    return alpha, shrink, beta, kappa, jnp.exp(mid), jnp.exp(last - mid), jnp.exp(last)
+
+
+def pair_products(x, y_hi, y_lo):
+    parts = [split2(keep(x, head)) for head in (0, 1)]
+    lhs = cat([cat([hi, lo], 1) for hi, lo in parts], 0)
+    return dot(lhs, cat([y_hi, y_hi], 0)) + dot(lhs[:, :128], y_lo)
+
+
+def pick(x):
+    first = (lax.broadcasted_iota(jnp.int32, (128, x.shape[1]), 1) & 127) < HD
+    return jnp.where(first, x[:128], x[128:])
 
 
 def inverses(lowers):
-    i, j = masks()
+    i = lax.broadcasted_iota(jnp.int32, (128, 128), 0)
+    j = lax.broadcasted_iota(jnp.int32, (128, 128), 1)
     apart = i ^ j
     eye = jnp.where(i == j, 1.0, 0.0)
-    zero = jnp.zeros((128, 256), bf16)
+    zero = jnp.zeros((128, 128), bf16)
     inv = [eye - jnp.where(apart == 1, low, zero).astype(f32) for low in lowers]
     for size in (2, 8, 32):
         inside = (apart >= size) & (apart < 4 * size)
-        inv_b = [block_diag(x.astype(bf16)) for x in inv]
-        steps = [block_diag(jnp.where(inside, low, zero)) for low in lowers]
-        hop = [dot(x.astype(bf16), c).astype(bf16) for x, c in zip(inv, steps)]
-        twice = [dot(h, block_diag(h)).astype(bf16) for h in hop]
-        once = [x - dot(h, b) for x, h, b in zip(inv, hop, inv_b)]
-        inv = [x + dot(t, block_diag(x.astype(bf16))) for x, t in zip(once, twice)]
+        inv_b = [x.astype(bf16) for x in inv]
+        hop = [
+            dot(x, jnp.where(inside, low, zero)).astype(bf16) for x, low in zip(inv_b, lowers)
+        ]
+        both = [dot(h, cat([h, x], 1)) for h, x in zip(hop, inv_b)]
+        once = [x - y[:, 128:] for x, y in zip(inv, both)]
+        inv = [x + dot(y[:, :128].astype(bf16), x.astype(bf16)) for x, y in zip(once, both)]
     return [x.astype(bf16) for x in inv]
 
 
-def stacked(x):
-    left, right = x[:, :128], x[:, 128:]
-    return cat([cat([keep(left, h), keep(right, h)], 1) for h in (0, 1)], 0)
-
-
 def solve_all(invs, lows, sides):
-    first = [dot(inv, stacked(side.astype(bf16))).astype(bf16) for inv, side in zip(invs, sides)]
-    back = [dot(low, stacked(x)) for low, x in zip(lows, first)]
+    first = [pick(dot(inv, side.astype(bf16))).astype(bf16) for inv, side in zip(invs, sides)]
+    back = [pick(dot(low, x)) for low, x in zip(lows, first)]
     miss = [
         (side - x.astype(f32) - y).astype(bf16) for side, x, y in zip(sides, first, back)
     ]
-    return [x.astype(f32) + dot(inv, stacked(m)) for x, inv, m in zip(first, invs, miss)]
+    return [x.astype(f32) + pick(dot(inv, m)) for x, inv, m in zip(first, invs, miss)]
 
 
 def maps_of(z, value, beta_end, kappa_end, gain_end):
@@ -184,29 +172,24 @@
     return dot(cat([hi, lo], 1), cat([weights, weights], 0))
 
 
-def recurrent_of(reads, state, local):
-    hi, lo = split2(reads)
-    weights = two_heads(state)
-    return dot_nt(cat([hi, lo], 1), cat([weights, weights], 1)) + local
-
-
-def head_norm(rec, gain, gate):
+def state_reads(reads, state):
+    both = dot_nt(cat(split2(reads), 0), two_heads(state))
+    return both[:128] + both[128:]
+
+
+def head_mean(x):
     ones = block_ones()
     ones2 = cat([ones, ones], 0)
-    offs = range(0, RCOLS, 128)
-    total = cat([head_sums(rec[:, o : o + 128], ones2) for o in offs], 1)
-    centred = rec - total * (1.0 / HD)
-    squares = centred * centred
-    spread = cat([head_sums(squares[:, o : o + 128], ones2) for o in offs], 1) * (1.0 / HD)
-    return (centred * lax.rsqrt(spread + 1.0) * gain * gate * sig(gate)).astype(bf16)
+    parts = [head_sums(x[:, o : o + 128], ones2) for o in range(0, x.shape[1], 128)]
+    return cat(parts, 1) * (1.0 / HD)
 
 
 def kernel(
     tok, gain, wr, wk, wv, wd, wa, wg, wp, wgp, dbase, rbase, hgain, mix, pscale, wor, wop, init,
     out,
     tok_v, gain_v, weight_v, acc_v, proj_v, norm_v, base_v, mix_v, pscale_v, wout_v, init_v,
-    pool_v, keys_v, low_v, side_v, z_v, reads_v, local_v, map_v, maps_in,
-    state_v, states_in, merged_v, recout_v, part_v, part_in, part_own, out_v,
+    scale_v, pool_v, keys_v, turn_v, low_v, side_v, z_v, reads_v, local_v, map_v, maps_in,
+    gate_v, state_v, states_in, merged_v, recout_v, part_v, part_in, part_own, out_v,
     w_sem, small_sem, tok_send, tok_recv, halo_send, halo_recv, map_send, map_recv,
     st_send, st_recv, part_send, part_recv, out_sem,
 ):
@@ -249,7 +232,7 @@
                 weight_v.at[half, :, pl.ds(OFFS[i], WIDTHS[i])],
                 w_sem.at[half, i],
             )
-            for i, w in enumerate(weights)
+            for i, w in ((i, weights[i]) for i in NEED)
         ]
         for half, at in ((0, mine), (1, theirs))
     ]
@@ -258,70 +241,51 @@
             copy.start()
 
     start(small[:3])
-    start(loads[0][:4])
+    start(loads[0][:2])
 
     def take(half):
         wide = tok_v[half].reshape(TOK, HALF).astype(f32)
         norm_v[half] = (wide * gain_v[half]).astype(bf16)
         return jnp.sum(wide * wide, axis=1, keepdims=True)
 
-    for copy in small[:2]:
-        copy.wait()
-    start(loads[0][4:] + loads[1][:2])
+    small[0].wait()
+    start(loads[0][2:4] + loads[1][:4] + small[3:5])
+    pl.semaphore_wait(barrier, N_SP)
+    send_tok = pltpu.make_async_remote_copy(
+        src_ref=tok_v.at[0],
+        dst_ref=tok_v.at[1],
+        send_sem=tok_send,
+        recv_sem=tok_recv,
+        device_id={"tp": other},
+        device_id_type=MESH,
+    )
+    send_tok.start()
+    small[1].wait()
     squares = take(0)
 
-    def columns(step):
-        return slice(768 * step, min(768 * step + 768, COLS))
-
-    for step in range(4):
+    early = (slice(0, EARLY // 2), slice(EARLY // 2, EARLY))
+    for step, at in enumerate(early):
         for copy in loads[0][2 * step : 2 * step + 2]:
             copy.wait()
-        at = columns(step)
         acc_v[:, at] = dot(norm_v[0], weight_v[0, :, at])
-        start((loads[1][2:4], loads[1][4:], small[3:], [])[step])
         if step == 0:
-            pl.semaphore_wait(barrier, N_SP)
-            send_tok = pltpu.make_async_remote_copy(
-                src_ref=tok_v.at[0],
-                dst_ref=tok_v.at[1],
-                send_sem=tok_send,
-                recv_sem=tok_recv,
-                device_id={"tp": other},
-                device_id_type=MESH,
-            )
-            send_tok.start()
+            start(loads[0][4:] + loads[1][4:] + small[5:])
 
     send_tok.wait_recv()
     small[2].wait()
     squares = squares + take(1)
-    scale = lax.rsqrt(squares * (1.0 / D) + 0.25)
-    for step in range(4):
+    scale_v[...] = jnp.broadcast_to(lax.rsqrt(squares * (1.0 / D) + 0.25), (TOK, 128))
+
+    def scaled(total):
+        return (total * cat([scale_v[...]] * (total.shape[1] // 128), 1)).astype(bf16)
+
+    for step, at in enumerate(early):
         for copy in loads[1][2 * step : 2 * step + 2]:
             copy.wait()
-        at = columns(step)
         total = acc_v[:, at] + dot(norm_v[1], weight_v[1, :, at])
-        proj_v[:, at] = (total * scale).astype(bf16)
-
-    for b in range(SEQ):
-        pool_v[b, 16:, :] = proj_v[b * ROWS : (b + 1) * ROWS, OFFS[6] : OFFS[7]]
-    halo = pltpu.make_async_remote_copy(
-        src_ref=pool_v.at[:, pl.ds(ROWS, 16), :],
-        dst_ref=pool_v.at[:, pl.ds(0, 16), :],
-        send_sem=halo_send,
-        recv_sem=halo_recv,
-        device_id={"sp": lax.rem(sp + 1, N_SP)},
-        device_id_type=MESH,
-    )
-
-    @pl.when(sp < N_SP - 1)
-    def _():
-        halo.start()
-
-    @pl.when(sp == 0)
-    def _():
-        pool_v[:, 0:16, :] = jnp.zeros((SEQ, 16, PCOLS), bf16)
-
-    for copy in small[3:6]:
+        proj_v[:, at] = scaled(total)
+
+    for copy in small[3:5]:
         copy.wait()
     groups = [(b, p) for b in range(SEQ) for p in range(PAIRS)]
 
@@ -329,9 +293,10 @@
         at = OFFS[index] + 128 * p
         return proj_v[b * ROWS : (b + 1) * ROWS, at : at + 128]
 
-    i2, j2 = masks()
-    strict = i2 > j2
-    inclusive = i2 >= j2
+    row = lax.broadcasted_iota(jnp.int32, (256, 128), 0) & 127
+    col = lax.broadcasted_iota(jnp.int32, (256, 128), 1)
+    strict = row > col
+    inclusive = row >= col
 
     def rows_of(index, b):
         at = OFFS[index]
@@ -342,11 +307,11 @@
 
     ends = []
     for b in range(SEQ):
-        alpha, rho, beta, kappa, e_mid, e_tail, e_last = prepare(
-            rows_of(0, b), rows_of(1, b), rows_of(3, b), rows_of(4, b), local_row(0), local_row(1)
+        alpha, shrink, beta, kappa, e_mid, e_tail, e_last = prepare(
+            rows_of(1, b), rows_of(3, b), rows_of(4, b), local_row(0), local_row(1)
         )
         keys_v[b, 0] = alpha
-        keys_v[b, 1] = rho
+        keys_v[b, 1] = shrink
         keys_v[b, 2] = beta
         keys_v[b, 3] = kappa
         ends.append((e_mid, e_tail, e_last))
@@ -361,12 +326,17 @@
 
     every = range(GROUPS)
     for g in every:
-        pairs = pair_products(pair_of(0, g), pair_of(2, g), pair_of(3, g))
-        low_v[g] = jnp.where(strict, pairs[:, :256], 0.0).astype(bf16)
-        cross = jnp.where(strict, pairs[:, 256:], 0.0).astype(bf16)
+        turned = cat([pair_of(2, g).T, pair_of(3, g).T], 1)
+        y_hi, y_lo = split2(turned)
+        turn_v[g, 0] = y_hi
+        turn_v[g, 1] = y_lo
+        pairs = pair_products(pair_of(0, g), y_hi, y_lo)
+        low_v[g] = jnp.where(strict, pairs[:, :128], 0.0).astype(bf16)
+        cross = jnp.where(strict, pairs[:, 128:], 0.0).astype(bf16)
         side_v[g, :, :128] = pair_of(0, g) * end_of(0, g)
-        side_v[g, :, 128:] = dot(cross, two_heads(part(2, *groups[g])))
-    invs = inverses([low_v[g] for g in every])
+        side_v[g, :, 128:] = pick(dot(cross, part(2, *groups[g])))
+    by_head = inverses([low_v[g, 128 * h : 128 * h + 128, :] for g in every for h in (0, 1)])
+    invs = [cat(by_head[2 * g : 2 * g + 2], 0) for g in every]
     map_copies = []
     for some in (range(0, 3), range(3, 6)):
         solved = solve_all(
@@ -400,35 +370,36 @@
             def _():
                 pltpu.make_async_copy(map_v.at[g], maps_in.at[sp], map_recv.at[sp]).start()
 
-    for copy in small[6:]:
+    def late(index, copies, at):
+        for half in (0, 1):
+            for copy in loads[half][copies]:
+                copy.wait()
+        total = dot(norm_v[0], weight_v[0, :, at]) + dot(norm_v[1], weight_v[1, :, at])
+        proj_v[:, at] = scaled(total)
+
+    late(6, slice(6, 8), slice(OFFS[6], COLS))
+    for b in range(SEQ):
+        pool_v[b, 16:, :] = proj_v[b * ROWS : (b + 1) * ROWS, OFFS[6] : OFFS[7]]
+    halo = pltpu.make_async_remote_copy(
+        src_ref=pool_v.at[:, pl.ds(ROWS, 16), :],
+        dst_ref=pool_v.at[:, pl.ds(0, 16), :],
+        send_sem=halo_send,
+        recv_sem=halo_recv,
+        device_id={"sp": lax.rem(sp + 1, N_SP)},
+        device_id_type=MESH,
+    )
+
+    @pl.when(sp < N_SP - 1)
+    def _():
+        halo.start()
+
+    @pl.when(sp == 0)
+    def _():
+        pool_v[:, 0:16, :] = jnp.zeros((SEQ, 16, PCOLS), bf16)
+
+    late(0, slice(4, 6), slice(OFFS[0], OFFS[6]))
+    for copy in small[5:]:
         copy.wait()
-
-    @pl.when(sp > 0)
-    def _():
-        halo.wait_recv()
-
-    places = (sp * ROWS + 1 + lax.broadcasted_iota(jnp.int32, (ROWS, 128), 0)).astype(f32)
-    for b in range(SEQ):
-        outs = []
-        for s in range(2):
-            at = slice(128 * s, 128 * s + 128)
-            own = pool_v[b, :, at].astype(f32)
-            total = own + pltpu.roll(own, 1, 0)
-            if s == 1:
-                total = total + pltpu.roll(total, 2, 0)
-            wide = total + pltpu.roll(total, 2 if s == 0 else 4, 0)
-            wide = wide + pltpu.roll(wide, 4 if s == 0 else 8, 0)
-            trail = jnp.where(tp == 0, total, wide)[16:]
-            window = jnp.where(tp == 0, float(2 << s), float(8 << s))
-            diff = (trail / jnp.minimum(places, window) - own[16:]).astype(bf16)
-            pooled = dot(diff, mix_v[s])
-            gate = proj_v[b * ROWS : (b + 1) * ROWS, OFFS[7] + 128 * s : OFFS[7] + 128 * s + 128]
-            gate = gate.astype(f32)
-            outs.append((pooled * pscale_v[:, at] * (gate * sig(gate))).astype(bf16))
-        recout_v[b * ROWS : (b + 1) * ROWS, RCOLS:] = cat(outs, 1)
-
-    for at in (slice(0, 1024), slice(1024, D)):
-        merged_v[:, at] = dot(recout_v[:, RCOLS:], wout_v[RCOLS:, at])
 
     def send_state(j):
         return pltpu.make_async_remote_copy(
@@ -442,6 +413,9 @@
 
     def wait_map(j):
         pltpu.make_async_copy(map_v.at[0], maps_in.at[j], map_recv.at[j]).wait()
+
+    def centred(state):
+        return (state - jnp.mean(state, axis=0, keepdims=True)).astype(bf16)
 
     @pl.when(is_owner)
     def _():
@@ -464,10 +438,10 @@
                     held.append(moved + cat([zero, maps_in[j, 1].astype(f32)], 0))
         for block in range(4):
             held = prefixes[block]
-            state_v[4 * block] = state.astype(bf16)
+            state_v[4 * block] = centred(state)
             for y in (1, 2, 3):
                 inside = held[y - 1]
-                state_v[4 * block + y] = after(state, inside[:HD], inside[HD:]).astype(bf16)
+                state_v[4 * block + y] = centred(after(state, inside[:HD], inside[HD:]))
             if block < 3:
                 state = after(state, held[3][:HD], held[3][HD:])
 
@@ -484,21 +458,54 @@
                 ).start()
 
     for g in every:
-        pairs = pair_products(pair_of(1, g), pair_of(2, g), pair_of(3, g))
-        within_beta = jnp.where(inclusive, pairs[:, :256], 0.0).astype(bf16)
-        within_kappa = jnp.where(inclusive, pairs[:, 256:], 0.0).astype(bf16)
-        drop = dot(within_beta, stacked(z_v[g]))
-        reads_v[g] = pair_of(1, g) * end_of(0, g) - drop[:, :128]
-        local_v[g] = dot(within_kappa, two_heads(part(2, *groups[g]))) - drop[:, 128:]
-
+        rho = part(0, *groups[g]).astype(f32) * pair_of(1, g)
+        pairs = pair_products(rho, turn_v[g, 0], turn_v[g, 1])
+        within_beta = jnp.where(inclusive, pairs[:, :128], 0.0).astype(bf16)
+        within_kappa = jnp.where(inclusive, pairs[:, 128:], 0.0).astype(bf16)
+        drop = pick(dot(within_beta, z_v[g]))
+        reads_v[g] = rho * end_of(0, g) - drop[:, :128]
+        local = pick(dot(within_kappa, part(2, *groups[g]))) - drop[:, 128:]
+        local_v[g] = local - head_mean(local)
     for b in range(SEQ):
-        recs = []
-        for g in range(PAIRS * b, PAIRS * b + PAIRS):
-            pltpu.make_async_copy(state_v.at[0], states_in.at[g], st_recv.at[g]).wait()
-            recs.append(recurrent_of(reads_v[g], states_in[g], local_v[g]))
-        recout_v[b * ROWS : (b + 1) * ROWS, :RCOLS] = head_norm(
-            cat(recs, 1), local_row(2), rows_of(5, b)
-        )
+        gate = rows_of(5, b)
+        gate_v[b] = local_row(2) * (gate * sig(gate))
+
+    @pl.when(sp > 0)
+    def _():
+        halo.wait_recv()
+
+    places = (sp * ROWS + 1 + lax.broadcasted_iota(jnp.int32, (ROWS, 128), 0)).astype(f32)
+    for b in range(SEQ):
+        outs = []
+        for s in range(2):
+            at = slice(128 * s, 128 * s + 128)
+            own = pool_v[b, :, at].astype(f32)
+            total = own + pltpu.roll(own, 1, 0)
+            if s == 1:
+                total = total + pltpu.roll(total, 2, 0)
+            wide = total + pltpu.roll(total, 2 if s == 0 else 4, 0)
+            wide = wide + pltpu.roll(wide, 4 if s == 0 else 8, 0)
+            trail = jnp.where(tp == 0, total, wide)[16:]
+            window = jnp.where(tp == 0, float(2 << s), float(8 << s))
+            diff = (trail / jnp.minimum(places, window) - own[16:]).astype(bf16)
+            pooled = dot(diff, mix_v[s])
+            gate = proj_v[b * ROWS : (b + 1) * ROWS, OFFS[7] + 128 * s : OFFS[7] + 128 * s + 128]
+            gate = gate.astype(f32)
+            outs.append((pooled * pscale_v[:, at] * (gate * sig(gate))).astype(bf16))
+        recout_v[b * ROWS : (b + 1) * ROWS, RCOLS:] = cat(outs, 1)
+
+    for at in (slice(0, 1024), slice(1024, D)):
+        merged_v[:, at] = dot(recout_v[:, RCOLS:], wout_v[RCOLS:, at])
+
+    for g in every:
+        pltpu.make_async_copy(state_v.at[0], states_in.at[g], st_recv.at[g]).wait()
+    centre = [state_reads(reads_v[g], states_in[g]) + local_v[g] for g in every]
+    for b in range(SEQ):
+        rec = cat(centre[PAIRS * b : PAIRS * b + PAIRS], 1)
+        spread = head_mean(rec * rec)
+        recout_v[b * ROWS : (b + 1) * ROWS, :RCOLS] = (
+            rec * lax.rsqrt(spread + 1.0) * gate_v[b]
+        ).astype(bf16)
 
     def product(at):
         return (merged_v[:, at] + dot(recout_v[:, :RCOLS], wout_v[:RCOLS, at])).astype(bf16)
@@ -563,7 +570,7 @@
         vmem((2, SEQ, ROWS, HALF), bf16),
         vmem((2, 1, HALF), f32),
         vmem((2, HALF, COLS), bf16),
-        vmem((TOK, COLS), f32),
+        vmem((TOK, EARLY), f32),
         vmem((TOK, COLS), bf16),
         vmem((2, TOK, HALF), bf16),
         vmem((3, 6, 128), f32),
@@ -571,15 +578,18 @@
         vmem((1, PCOLS), f32),
         vmem((RCOLS + PCOLS, D), bf16),
         vmem((SEQ, 2 * PAIRS, HD, HD), f32),
+        vmem((TOK, 128), f32),
         vmem((SEQ, 16 + ROWS, PCOLS), bf16),
         vmem((SEQ, 4, ROWS, RCOLS), f32),
-        vmem((GROUPS, 128, 256), bf16),
+        vmem((GROUPS, 2, 128, 256), bf16),
+        vmem((GROUPS, 256, 128), bf16),
         vmem((GROUPS, 128, 256), f32),
         vmem((GROUPS, 128, 256), bf16),
         vmem((GROUPS, 128, 128), f32),
         vmem((GROUPS, 128, 128), f32),
         vmem((GROUPS, 2, HD, 128), bf16),
         vmem((N_SP, 2, HD, 128), bf16),
+        vmem((SEQ, ROWS, RCOLS), f32),
         vmem((N_SP, HD, 128), bf16),
         vmem((GROUPS, HD, 128), bf16),
         vmem((TOK, D), f32),

time: 36 us -> 33.9 us (0.942)
  Pallas kernels: 33.9 us -> 31.9 us
    pallas_call x1, Pallas kernels: 33.9 us -> 31.9 us  [shards(): pl.pallas_call(kernel, out_shape=jax.ShapeDtypeStruct((SEQ, ROWS, HALF),...]
where the time goes in v2:
time: 33.9 us; the launch traced here: 33.8 us
  Pallas kernels  31.9 us (94%)
  local copies, waits for them, and re-layouts  1.87 us (6%)
    pallas_call x1, Pallas kernels, shards(): pl.pallas_call(kernel, out_shape=jax.ShapeDtypeStruct((SEQ, ROWS, HALF),...  31.9 us
    unnamed x1, local copies, waits for them, and re-layouts  1.87 us

profile of v2, /device:TPU:1, one launch (start us, length us, event | category | flops | bytes accessed | tf_op | source)
XLA Modules:
  0.0 33.8 jit_solution(3113756499513005191)
XLA Ops:
  0.0 31.9 %layer.1 = bf16[2,128,1024]{2,1,0:T(8,128)(2,1)} custom-call(bf16[2,128,1024]{2,1,0:T(8,128)(2,1)} %tok.1, f32[1,2048]{1,0:T(1,128)} %bitcast.5, bf16[2048,384]{1,0:T(8,128)(2,1)} %wr.1, bf16[2048,384]{1,0:T(8,128)(2,1)} %wk.1, bf16[2048,384]{1,0:T(8,128)(2,1)} %wv.1, bf16[2048,384]{1,0:T(8,128)(2,1)} %wd.1, bf16[2048,384]{1,0:T(8,128)(2,1)} %wa.1, ...), custom_call_target="tpu_custom_call" | custom-call | tf_op jit(solution)/shard_map/layer/pallas_call | solution.py:615
  31.9 1.9 %copy.20 = bf16[2,128,1024]{2,1,0:T(8,128)(2,1)} copy(bf16[2,128,1024]{2,1,0:T(8,128)(2,1)} %layer.1) | data formatting | bytes 1048576

commit v3 on v2

--- a/solution.py
+++ b/solution.py
@@ -186,44 +186,53 @@
 
 def kernel(
     tok, gain, wr, wk, wv, wd, wa, wg, wp, wgp, dbase, rbase, hgain, mix, pscale, wor, wop, init,
-    out,
-    tok_v, gain_v, weight_v, acc_v, proj_v, norm_v, base_v, mix_v, pscale_v, wout_v, init_v,
+    own_out, arrived_out,
+    tok_v, gain_v, weight_v, acc_v, proj_v, norm_v, square_v, base_v, mix_v, pscale_v, wout_v, init_v, init_in,
     scale_v, pool_v, keys_v, turn_v, low_v, side_v, z_v, reads_v, local_v, map_v, maps_in,
-    gate_v, state_v, states_in, merged_v, recout_v, part_v, part_in, part_own, out_v,
+    gate_v, state_v, states_in, merged_v, recout_v, part_v, part_own,
     w_sem, small_sem, tok_send, tok_recv, halo_send, halo_recv, map_send, map_recv,
-    st_send, st_recv, part_send, part_recv, out_sem,
+    st_send, st_recv, part_send, part_recv, own_sem, init_send, init_recv,
 ):
     sp = lax.axis_index("sp")
     tp = lax.axis_index("tp")
     other = 1 - tp
     weights = (wr, wk, wv, wd, wa, wg, wp, wgp)
     group_of = lax.div(sp, 2)
-    is_owner = (lax.rem(sp, 2) == tp) & (sp < 2 * GROUPS)
+    side = lax.rem(sp, 2)
+    is_owner = (tp == 1) & (sp < 2 * GROUPS)
+    gives_init = (tp == 0) & (side == 0) & (sp < 2 * GROUPS)
+    keeps_init = (tp == 1) & (side == 1) & (sp < 2 * GROUPS)
 
     barrier = pltpu.get_barrier_semaphore()
     pl.semaphore_signal(barrier, inc=1, device_id={"tp": other}, device_id_type=MESH)
 
     @pl.loop(1, N_SP)
     def _(step):
-        pl.semaphore_signal(
-            barrier, inc=1, device_id={"sp": lax.rem(sp + step, N_SP)}, device_id_type=MESH
-        )
+        peer = lax.rem(sp + step, N_SP)
+        for core in (0, 1):
+            pl.semaphore_signal(
+                barrier, inc=1, device_id={"sp": peer, "tp": core}, device_id_type=MESH
+            )
 
     mine = pl.multiple_of(tp * HALF, HALF)
     theirs = pl.multiple_of(other * HALF, HALF)
     pool_at = pl.multiple_of(tp * PCOLS, 128)
+    held = jnp.minimum(group_of, GROUPS - 1)
     small = [
-        pltpu.make_async_copy(tok, tok_v.at[0], small_sem.at[0]),
-        pltpu.make_async_copy(gain.at[:, pl.ds(mine, HALF)], gain_v.at[0], small_sem.at[1]),
-        pltpu.make_async_copy(gain.at[:, pl.ds(theirs, HALF)], gain_v.at[1], small_sem.at[2]),
-        pltpu.make_async_copy(dbase, base_v.at[0], small_sem.at[3]),
-        pltpu.make_async_copy(rbase, base_v.at[1], small_sem.at[4]),
-        pltpu.make_async_copy(hgain, base_v.at[2], small_sem.at[5]),
-        pltpu.make_async_copy(mix.at[pl.ds(tp * 2, 2)], mix_v, small_sem.at[6]),
-        pltpu.make_async_copy(pscale.at[:, pl.ds(pool_at, PCOLS)], pscale_v, small_sem.at[7]),
-        pltpu.make_async_copy(init, init_v, small_sem.at[8]),
-        pltpu.make_async_copy(wor, wout_v.at[pl.ds(0, RCOLS)], small_sem.at[9]),
-        pltpu.make_async_copy(wop, wout_v.at[pl.ds(RCOLS, PCOLS)], small_sem.at[10]),
+        pltpu.make_async_copy(tok, tok_v, small_sem.at[0]),
+        pltpu.make_async_copy(gain.at[:, pl.ds(mine, HALF)], gain_v, small_sem.at[1]),
+        pltpu.make_async_copy(dbase, base_v.at[0], small_sem.at[2]),
+        pltpu.make_async_copy(rbase, base_v.at[1], small_sem.at[3]),
+        pltpu.make_async_copy(hgain, base_v.at[2], small_sem.at[4]),
+        pltpu.make_async_copy(mix.at[pl.ds(tp * 2, 2)], mix_v, small_sem.at[5]),
+        pltpu.make_async_copy(pscale.at[:, pl.ds(pool_at, PCOLS)], pscale_v, small_sem.at[6]),
+        pltpu.make_async_copy(
+            init.at[lax.div(held, PAIRS), pl.ds(2 * lax.rem(held, PAIRS), 2)],
+            init_v,
+            small_sem.at[7],
+        ),
+        pltpu.make_async_copy(wor, wout_v.at[pl.ds(0, RCOLS)], small_sem.at[8]),
+        pltpu.make_async_copy(wop, wout_v.at[pl.ds(RCOLS, PCOLS)], small_sem.at[9]),
     ]
     loads = [
         [
@@ -240,41 +249,39 @@
         for copy in copies:
             copy.start()
 
-    start(small[:3])
+    start(small[:2])
     start(loads[0][:2])
 
-    def take(half):
-        wide = tok_v[half].reshape(TOK, HALF).astype(f32)
-        norm_v[half] = (wide * gain_v[half]).astype(bf16)
-        return jnp.sum(wide * wide, axis=1, keepdims=True)
-
     small[0].wait()
-    start(loads[0][2:4] + loads[1][:4] + small[3:5])
-    pl.semaphore_wait(barrier, N_SP)
-    send_tok = pltpu.make_async_remote_copy(
-        src_ref=tok_v.at[0],
-        dst_ref=tok_v.at[1],
-        send_sem=tok_send,
-        recv_sem=tok_recv,
-        device_id={"tp": other},
-        device_id_type=MESH,
-    )
-    send_tok.start()
+    start(loads[0][2:4] + loads[1][:4] + small[2:4])
     small[1].wait()
-    squares = take(0)
-
+    wide = tok_v[...].reshape(TOK, HALF).astype(f32)
+    norm_v[0] = (wide * gain_v[...]).astype(bf16)
+    squares = wide * wide
+    square_v[0] = sum(squares[:, o : o + 128] for o in range(0, HALF, 128))
+
+    pl.semaphore_wait(barrier, 2 * N_SP - 1)
+    send_tok = [
+        pltpu.make_async_remote_copy(
+            src_ref=ref.at[0],
+            dst_ref=ref.at[1],
+            send_sem=tok_send.at[i],
+            recv_sem=tok_recv.at[i],
+            device_id={"tp": other},
+            device_id_type=MESH,
+        )
+        for i, ref in enumerate((norm_v, square_v))
+    ]
+    start(send_tok)
     early = (slice(0, EARLY // 2), slice(EARLY // 2, EARLY))
     for step, at in enumerate(early):
         for copy in loads[0][2 * step : 2 * step + 2]:
             copy.wait()
         acc_v[:, at] = dot(norm_v[0], weight_v[0, :, at])
         if step == 0:
-            start(loads[0][4:] + loads[1][4:] + small[5:])
-
-    send_tok.wait_recv()
-    small[2].wait()
-    squares = squares + take(1)
-    scale_v[...] = jnp.broadcast_to(lax.rsqrt(squares * (1.0 / D) + 0.25), (TOK, 128))
+            start(loads[0][4:] + loads[1][4:] + small[4:])
+
+    send_tok[0].wait_recv()
 
     def scaled(total):
         return (total * cat([scale_v[...]] * (total.shape[1] // 128), 1)).astype(bf16)
@@ -283,9 +290,14 @@
         for copy in loads[1][2 * step : 2 * step + 2]:
             copy.wait()
         total = acc_v[:, at] + dot(norm_v[1], weight_v[1, :, at])
+        if step == 0:
+            send_tok[1].wait_recv()
+            squares = jnp.sum(square_v[0] + square_v[1], axis=1, keepdims=True)
+            scale = lax.rsqrt(squares * (1.0 / D) + 0.25)
+            scale_v[...] = jnp.broadcast_to(scale, (TOK, 128))
         proj_v[:, at] = scaled(total)
 
-    for copy in small[3:5]:
+    for copy in small[2:4]:
         copy.wait()
     groups = [(b, p) for b in range(SEQ) for p in range(PAIRS)]
 
@@ -338,37 +350,34 @@
     by_head = inverses([low_v[g, 128 * h : 128 * h + 128, :] for g in every for h in (0, 1)])
     invs = [cat(by_head[2 * g : 2 * g + 2], 0) for g in every]
     map_copies = []
-    for some in (range(0, 3), range(3, 6)):
-        solved = solve_all(
-            [invs[g] for g in some], [low_v[g] for g in some], [side_v[g] for g in some]
+    solved = solve_all(invs, [low_v[g] for g in every], [side_v[g] for g in every])
+    for g, z in zip(every, solved):
+        z_v[g] = z.astype(bf16)
+        tail = end_of(1, g)
+        transit, written = maps_of(
+            z, part(2, *groups[g]), pair_of(2, g) * tail, pair_of(3, g) * tail, end_of(2, g)
         )
-        for g, z in zip(some, solved):
-            z_v[g] = z.astype(bf16)
-            tail = end_of(1, g)
-            transit, written = maps_of(
-                z, part(2, *groups[g]), pair_of(2, g) * tail, pair_of(3, g) * tail, end_of(2, g)
-            )
-            map_v[g, 0] = transit
-            map_v[g, 1] = written
-        for g in some:
-            owner = 2 * g + tp
-            copy = pltpu.make_async_remote_copy(
-                src_ref=map_v.at[g],
-                dst_ref=maps_in.at[sp],
-                send_sem=map_send.at[g],
-                recv_sem=map_recv.at[sp],
-                device_id={"sp": owner},
-                device_id_type=MESH,
-            )
-            map_copies.append(copy)
-
-            @pl.when((sp != owner) & (sp < N_SP - 1))
-            def _():
-                copy.start()
-
-            @pl.when(sp == owner)
-            def _():
-                pltpu.make_async_copy(map_v.at[g], maps_in.at[sp], map_recv.at[sp]).start()
+        map_v[g, 0] = transit
+        map_v[g, 1] = written
+    own_map = [(tp == 1) & (sp == 2 * g + 1) for g in every]
+    for g in every:
+        copy = pltpu.make_async_remote_copy(
+            src_ref=map_v.at[g],
+            dst_ref=maps_in.at[sp],
+            send_sem=map_send.at[g],
+            recv_sem=map_recv.at[sp],
+            device_id={"sp": 2 * g + tp, "tp": 1},
+            device_id_type=MESH,
+        )
+        map_copies.append(copy)
+
+        @pl.when(jnp.logical_not(own_map[g]) & (sp < N_SP - 1))
+        def _():
+            copy.start()
+
+        @pl.when(own_map[g])
+        def _():
+            pltpu.make_async_copy(map_v.at[g], maps_in.at[sp], map_recv.at[sp]).start()
 
     def late(index, copies, at):
         for half in (0, 1):
@@ -397,17 +406,13 @@
     def _():
         pool_v[:, 0:16, :] = jnp.zeros((SEQ, 16, PCOLS), bf16)
 
-    late(0, slice(4, 6), slice(OFFS[0], OFFS[6]))
-    for copy in small[5:]:
-        copy.wait()
-
     def send_state(j):
         return pltpu.make_async_remote_copy(
             src_ref=state_v.at[j],
             dst_ref=states_in.at[group_of],
             send_sem=st_send.at[j],
             recv_sem=st_recv.at[group_of],
-            device_id={"sp": j},
+            device_id={"sp": j, "tp": side},
             device_id_type=MESH,
         )
 
@@ -417,45 +422,72 @@
     def centred(state):
         return (state - jnp.mean(state, axis=0, keepdims=True)).astype(bf16)
 
+    small[7].wait()
+    give = pltpu.make_async_remote_copy(
+        src_ref=init_v,
+        dst_ref=init_in,
+        send_sem=init_send,
+        recv_sem=init_recv,
+        device_id={"tp": other},
+        device_id_type=MESH,
+    )
+
+    @pl.when(gives_init)
+    def _():
+        give.start()
+
+    @pl.when(keeps_init)
+    def _():
+        pltpu.make_async_copy(init_v, init_in, init_recv).start()
+
     @pl.when(is_owner)
     def _():
-        seq = lax.div(group_of, PAIRS)
-        pair = lax.rem(group_of, PAIRS)
-        state = cat([init_v[seq, 2 * pair], init_v[seq, 2 * pair + 1]], 1)
+        pltpu.make_async_copy(init_v, init_in, init_recv).wait()
+        start_state = cat([init_in[0], init_in[1]], 1)
         for j in range(N_SP - 1):
             wait_map(j)
         zero = jnp.zeros((HD, 128), f32)
+
+        def then(left, transit, written):
+            return after_given(left, transit) + cat([zero, written.astype(f32)], 0)
+
+        def apply(state, held):
+            return after(state, held[:HD], held[HD:])
+
         prefixes = []
         for block in range(4):
-            held = [cat([maps_in[4 * block, 0], maps_in[4 * block, 1]], 0).astype(f32)]
-            prefixes.append(held)
+            prefixes.append([cat([maps_in[4 * block, 0], maps_in[4 * block, 1]], 0).astype(f32)])
         for y in (1, 2, 3):
             for block in range(4):
                 j = 4 * block + y
                 if j < N_SP - 1:
-                    held = prefixes[block]
-                    moved = after_given(held[-1], maps_in[j, 0])
-                    held.append(moved + cat([zero, maps_in[j, 1].astype(f32)], 0))
+                    prefixes[block].append(then(prefixes[block][-1], maps_in[j, 0], maps_in[j, 1]))
+        totals = [prefixes[block][3] for block in range(3)]
+        ahead = after(totals[1], totals[2][:HD], cat([zero, totals[2][HD:]], 0))
+        fourth = apply(start_state, totals[0])
+        starts = [start_state, fourth, apply(fourth, totals[1]), apply(fourth, ahead)]
         for block in range(4):
-            held = prefixes[block]
-            state_v[4 * block] = centred(state)
+            state_v[4 * block] = centred(starts[block])
             for y in (1, 2, 3):
-                inside = held[y - 1]
-                state_v[4 * block + y] = centred(after(state, inside[:HD], inside[HD:]))
-            if block < 3:
-                state = after(state, held[3][:HD], held[3][HD:])
+                inside = prefixes[block][y - 1]
+                moved = after_given(starts[block], inside[:HD].astype(bf16)) + inside[HD:]
+                state_v[4 * block + y] = centred(moved)
 
         @pl.loop(0, N_SP)
         def _(j):
-            @pl.when(j != sp)
+            @pl.when((j != sp) | (side == 0))
             def _():
                 send_state(j).start()
 
-            @pl.when(j == sp)
+            @pl.when((j == sp) & (side == 1))
             def _():
                 pltpu.make_async_copy(
                     state_v.at[j], states_in.at[group_of], st_recv.at[group_of]
                 ).start()
+
+    late(0, slice(4, 6), slice(OFFS[0], OFFS[6]))
+    for copy in small[4:7] + small[8:]:
+        copy.wait()
 
     for g in every:
         rho = part(0, *groups[g]).astype(f32) * pair_of(1, g)
@@ -508,55 +540,59 @@
         ).astype(bf16)
 
     def product(at):
-        return (merged_v[:, at] + dot(recout_v[:, :RCOLS], wout_v[:RCOLS, at])).astype(bf16)
+        total = merged_v[:, at] + dot(recout_v[:, :RCOLS], wout_v[:RCOLS, at])
+        return total.astype(bf16).reshape(SEQ, ROWS, 512)
+
+    def columns(ref, tile):
+        return ref.at[:, :, pl.ds(512 * tile, 512)]
 
     def send_part(tile):
         return pltpu.make_async_remote_copy(
             src_ref=part_v.at[tile],
-            dst_ref=part_in.at[tile],
+            dst_ref=columns(arrived_out, tile),
             send_sem=part_send.at[tile],
             recv_sem=part_recv.at[tile],
             device_id={"tp": other},
             device_id_type=MESH,
         )
 
-    def store_out(tile):
-        at = pl.ds(512 * tile, 512)
-        return pltpu.make_async_copy(out_v.at[:, :, at], out.at[:, :, at], out_sem.at[tile])
+    def keep_part(tile):
+        return pltpu.make_async_copy(part_own.at[tile], columns(own_out, tile), own_sem.at[tile])
 
     for tile in range(2):
         part_v[tile] = product(pl.ds(pl.multiple_of(theirs + tile * 512, 512), 512))
         send_part(tile).start()
     for tile in range(2):
         part_own[tile] = product(pl.ds(pl.multiple_of(mine + tile * 512, 512), 512))
-    for tile in range(2):
-        send_part(tile).wait_recv()
-        total = part_own[tile].astype(f32) + part_in[tile].astype(f32)
-        out_v[:, :, 512 * tile : 512 * tile + 512] = total.astype(bf16).reshape(SEQ, ROWS, 512)
-        store_out(tile).start()
-
-    send_tok.wait_send()
+        keep_part(tile).start()
+
+    for copy in send_tok:
+        copy.wait_send()
 
     @pl.when(sp < N_SP - 1)
     def _():
         halo.wait_send()
 
     for g, copy in enumerate(map_copies):
-        @pl.when((sp != 2 * g + tp) & (sp < N_SP - 1))
+        @pl.when(jnp.logical_not(own_map[g]) & (sp < N_SP - 1))
         def _():
             copy.wait_send()
 
+    @pl.when(gives_init)
+    def _():
+        give.wait_send()
+
     @pl.when(is_owner)
     def _():
         @pl.loop(0, N_SP)
         def _(j):
-            @pl.when(j != sp)
+            @pl.when((j != sp) | (side == 0))
             def _():
                 send_state(j).wait_send()
 
     for tile in range(2):
-        send_part(tile).wait_send()
-        store_out(tile).wait()
+        send_part(tile).wait()
+        keep_part(tile).wait()
 
 
 def shards(
@@ -567,17 +603,19 @@
     row = lambda x: x.reshape(1, -1)
     tile = lambda x: x.reshape(6, 128)
     scratch = [
-        vmem((2, SEQ, ROWS, HALF), bf16),
-        vmem((2, 1, HALF), f32),
+        vmem((SEQ, ROWS, HALF), bf16),
+        vmem((1, HALF), f32),
         vmem((2, HALF, COLS), bf16),
         vmem((TOK, EARLY), f32),
         vmem((TOK, COLS), bf16),
         vmem((2, TOK, HALF), bf16),
+        vmem((2, TOK, 128), f32),
         vmem((3, 6, 128), f32),
         vmem((2, 128, 128), bf16),
         vmem((1, PCOLS), f32),
         vmem((RCOLS + PCOLS, D), bf16),
-        vmem((SEQ, 2 * PAIRS, HD, HD), f32),
+        vmem((2, HD, HD), f32),
+        vmem((2, HD, HD), f32),
         vmem((TOK, 128), f32),
         vmem((SEQ, 16 + ROWS, PCOLS), bf16),
         vmem((SEQ, 4, ROWS, RCOLS), f32),
@@ -594,14 +632,12 @@
         vmem((GROUPS, HD, 128), bf16),
         vmem((TOK, D), f32),
         vmem((TOK, RCOLS + PCOLS), bf16),
-        vmem((2, TOK, 512), bf16),
-        vmem((2, TOK, 512), bf16),
-        vmem((2, TOK, 512), bf16),
-        vmem((SEQ, ROWS, HALF), bf16),
+        vmem((2, SEQ, ROWS, 512), bf16),
+        vmem((2, SEQ, ROWS, 512), bf16),
         sem((2, 8)),
-        sem((11,)),
-        sem,
-        sem,
+        sem((10,)),
+        sem((2,)),
+        sem((2,)),
         sem,
         sem,
         sem((GROUPS,)),
@@ -611,12 +647,14 @@
         sem((2,)),
         sem((2,)),
         sem((2,)),
+        sem,
+        sem,
     ]
-    return pl.pallas_call(
+    own, arrived = pl.pallas_call(
         kernel,
-        out_shape=jax.ShapeDtypeStruct((SEQ, ROWS, HALF), bf16),
+        out_shape=[jax.ShapeDtypeStruct((SEQ, ROWS, HALF), bf16)] * 2,
         in_specs=[pl.BlockSpec(memory_space=pl.ANY)] * 18,
-        out_specs=pl.BlockSpec(memory_space=pl.ANY),
+        out_specs=[pl.BlockSpec(memory_space=pl.ANY)] * 2,
         scratch_shapes=scratch,
         compiler_params=pltpu.CompilerParams(
             collective_id=0, has_side_effects=True, vmem_limit_bytes=56 << 20
@@ -627,6 +665,7 @@
         w_gate_pool, tile(decay_base), tile(rate_base), tile(head_gain), pool_mix, row(pool_scale),
         w_out_rec, w_out_pool, init_state,
     )
+    return (own.astype(f32) + arrived.astype(f32)).astype(bf16)
 
 
 def solution(mesh):

time: 33.9 us -> 32.5 us (0.959)
  other arithmetic: 0 us -> 2.19 us
  local copies, waits for them, and re-layouts: 1.87 us -> 0 us
  Pallas kernels: 31.9 us -> 30.2 us
    convert_element_type x0 -> x1, other arithmetic: none -> 2.19 us  [shards(): return (own.astype(f32) + arrived.astype(f32)).astype(bf16)]
    unnamed x1 -> x0, local copies, waits for them, and re-layouts: 1.87 us -> none
    pallas_call x1, Pallas kernels: 31.9 us -> 30.2 us  [shards(): pl.pallas_call(kernel, out_shape=[jax.ShapeDtypeStruct((SEQ, ROWS, HALF),...]
where the time goes in v3:
time: 32.5 us; the launch traced here: 32.4 us
  Pallas kernels  30.2 us (93%)
  other arithmetic  2.19 us (7%)
    pallas_call x1, Pallas kernels, shards(): pl.pallas_call(kernel, out_shape=[jax.ShapeDtypeStruct((SEQ, ROWS, HALF),...  30.2 us
    convert_element_type x1, other arithmetic, shards(): return (own.astype(f32) + arrived.astype(f32)).astype(bf16)  2.19 us

profile of v3, /device:TPU:1, one launch (start us, length us, event | category | flops | bytes accessed | tf_op | source)
XLA Modules:
  0.0 32.4 jit_solution(6509003284054627882)
XLA Ops:
  0.0 30.2 %layer.1 = (bf16[2,128,1024]{2,1,0:T(8,128)(2,1)}, bf16[2,128,1024]{2,1,0:T(8,128)(2,1)}) custom-call(bf16[2,128,1024]{2,1,0:T(8,128)(2,1)} %tok.1, f32[1,2048]{1,0:T(1,128)} %bitcast.5, bf16[2048,384]{1,0:T(8,128)(2,1)} %wr.1, bf16[2048,384]{1,0:T(8,128)(2,1)} %wk.1, bf16[2048,384]{1,0:T(8,128)(2,1)} %wv.1, bf16[2048,384]{1,0:T(8,128)(2,1)} %wd.1, ...), custom_call_target="tpu_custom_call" | custom-call | tf_op jit(solution)/shard_map/layer/pallas_call | solution.py:653
  30.2 2.2 %add_convert_fusion = bf16[2,128,1024]{2,1,0:T(8,128)(2,1)} fusion(bf16[2,128,1024]{2,1,0:T(8,128)(2,1)} %get-tuple-element.8, bf16[2,128,1024]{2,1,0:T(8,128)(2,1)} %get-tuple-element.7), kind=kLoop, calls=%fused_computation | loop fusion | flops 1048576 | bytes 1572864 | tf_op jit(solution)/shard_map/convert_element_type | solution.py:668

commit v4 on v3

--- a/solution.py
+++ b/solution.py
@@ -191,7 +191,7 @@
     scale_v, pool_v, keys_v, turn_v, low_v, side_v, z_v, reads_v, local_v, map_v, maps_in,
     gate_v, state_v, states_in, merged_v, recout_v, part_v, part_own,
     w_sem, small_sem, tok_send, tok_recv, halo_send, halo_recv, map_send, map_recv,
-    st_send, st_recv, part_send, part_recv, own_sem, init_send, init_recv,
+    st_send, st_recv, part_send, part_recv, own_sem, init_send, init_recv, pair_sem, go_sem,
 ):
     sp = lax.axis_index("sp")
     tp = lax.axis_index("tp")
@@ -204,15 +204,13 @@
     keeps_init = (tp == 1) & (side == 1) & (sp < 2 * GROUPS)
 
     barrier = pltpu.get_barrier_semaphore()
-    pl.semaphore_signal(barrier, inc=1, device_id={"tp": other}, device_id_type=MESH)
-
-    @pl.loop(1, N_SP)
-    def _(step):
-        peer = lax.rem(sp + step, N_SP)
-        for core in (0, 1):
-            pl.semaphore_signal(
-                barrier, inc=1, device_id={"sp": peer, "tp": core}, device_id_type=MESH
-            )
+
+    def tell(semaphore, **device):
+        pl.semaphore_signal(semaphore, inc=1, device_id=device, device_id_type=MESH)
+
+    @pl.when(tp == 1)
+    def _():
+        tell(barrier, tp=other)
 
     mine = pl.multiple_of(tp * HALF, HALF)
     theirs = pl.multiple_of(other * HALF, HALF)
@@ -253,6 +251,12 @@
     start(loads[0][:2])
 
     small[0].wait()
+
+    @pl.when(tp == 0)
+    def _():
+        pl.semaphore_wait(barrier, 1)
+        tell(pair_sem, tp=other)
+
     start(loads[0][2:4] + loads[1][:4] + small[2:4])
     small[1].wait()
     wide = tok_v[...].reshape(TOK, HALF).astype(f32)
@@ -260,7 +264,14 @@
     squares = wide * wide
     square_v[0] = sum(squares[:, o : o + 128] for o in range(0, HALF, 128))
 
-    pl.semaphore_wait(barrier, 2 * N_SP - 1)
+    @pl.when(tp == 1)
+    def _():
+        pl.semaphore_wait(pair_sem, 1)
+
+        @pl.loop(1, N_SP)
+        def _(step):
+            tell(barrier, sp=lax.rem(sp + step, N_SP))
+
     send_tok = [
         pltpu.make_async_remote_copy(
             src_ref=ref.at[0],
@@ -347,6 +358,11 @@
         cross = jnp.where(strict, pairs[:, 128:], 0.0).astype(bf16)
         side_v[g, :, :128] = pair_of(0, g) * end_of(0, g)
         side_v[g, :, 128:] = pick(dot(cross, part(2, *groups[g])))
+    @pl.when(tp == 1)
+    def _():
+        pl.semaphore_wait(barrier, N_SP - 1)
+        tell(go_sem, tp=other)
+
     by_head = inverses([low_v[g, 128 * h : 128 * h + 128, :] for g in every for h in (0, 1)])
     invs = [cat(by_head[2 * g : 2 * g + 2], 0) for g in every]
     map_copies = []
@@ -359,6 +375,10 @@
         )
         map_v[g, 0] = transit
         map_v[g, 1] = written
+    @pl.when(tp == 0)
+    def _():
+        pl.semaphore_wait(go_sem, 1)
+
     own_map = [(tp == 1) & (sp == 2 * g + 1) for g in every]
     for g in every:
         copy = pltpu.make_async_remote_copy(
@@ -649,6 +669,8 @@
         sem((2,)),
         sem,
         sem,
+        pltpu.SemaphoreType.REGULAR,
+        pltpu.SemaphoreType.REGULAR,
     ]
     own, arrived = pl.pallas_call(
         kernel,

time: 32.5 us -> 30 us (0.923)
  Pallas kernels: 30.2 us -> 27.7 us
    pallas_call x1, Pallas kernels: 30.2 us -> 27.7 us  [shards(): pl.pallas_call(kernel, out_shape=[jax.ShapeDtypeStruct((SEQ, ROWS, HALF),...]
where the time goes in v4:
time: 30 us; the launch traced here: 29.9 us
  Pallas kernels  27.7 us (92%)
  other arithmetic  2.19 us (7%)
    pallas_call x1, Pallas kernels, shards(): pl.pallas_call(kernel, out_shape=[jax.ShapeDtypeStruct((SEQ, ROWS, HALF),...  27.7 us
    convert_element_type x1, other arithmetic, shards(): return (own.astype(f32) + arrived.astype(f32)).astype(bf16)  2.19 us

profile of v4, /device:TPU:1, one launch (start us, length us, event | category | flops | bytes accessed | tf_op | source)
XLA Modules:
  0.0 29.9 jit_solution(5525224151181597417)
XLA Ops:
  0.0 27.7 %layer.1 = (bf16[2,128,1024]{2,1,0:T(8,128)(2,1)}, bf16[2,128,1024]{2,1,0:T(8,128)(2,1)}) custom-call(bf16[2,128,1024]{2,1,0:T(8,128)(2,1)} %tok.1, f32[1,2048]{1,0:T(1,128)} %bitcast.5, bf16[2048,384]{1,0:T(8,128)(2,1)} %wr.1, bf16[2048,384]{1,0:T(8,128)(2,1)} %wk.1, bf16[2048,384]{1,0:T(8,128)(2,1)} %wv.1, bf16[2048,384]{1,0:T(8,128)(2,1)} %wd.1, ...), custom_call_target="tpu_custom_call" | custom-call | tf_op jit(solution)/shard_map/layer/pallas_call | solution.py:675
  27.7 2.2 %add_convert_fusion = bf16[2,128,1024]{2,1,0:T(8,128)(2,1)} fusion(bf16[2,128,1024]{2,1,0:T(8,128)(2,1)} %get-tuple-element.8, bf16[2,128,1024]{2,1,0:T(8,128)(2,1)} %get-tuple-element.7), kind=kLoop, calls=%fused_computation | loop fusion | flops 1048576 | bytes 1572864 | tf_op jit(solution)/shard_map/convert_element_type | solution.py:690

commit v5 on v4

--- a/solution.py
+++ b/solution.py
@@ -158,18 +158,9 @@
     return transit.astype(bf16), (-packed[1]).astype(bf16)
 
 
-def after(left, transit, written):
-    l_hi, l_lo = split2(left)
-    t_hi, t_lo = split2(transit)
-    weights = two_heads(t_hi)
-    moved = dot(cat([l_hi, l_lo], 1), cat([weights, weights], 0)) + dot(l_hi, two_heads(t_lo))
-    return moved + written
-
-
-def after_given(left, transit):
-    hi, lo = split2(left)
-    weights = two_heads(transit)
-    return dot(cat([hi, lo], 1), cat([weights, weights], 0))
+def after_given(state, transit):
+    both = dot(cat(split2(state), 0), two_heads(transit))
+    return both[:HD] + both[HD:]
 
 
 def state_reads(reads, state):
@@ -426,6 +417,16 @@
     def _():
         pool_v[:, 0:16, :] = jnp.zeros((SEQ, 16, PCOLS), bf16)
 
+    late(0, slice(4, 5), slice(OFFS[0], OFFS[5]))
+    for g in every:
+        rho = part(0, *groups[g]).astype(f32) * pair_of(1, g)
+        pairs = pair_products(rho, turn_v[g, 0], turn_v[g, 1])
+        within_beta = jnp.where(inclusive, pairs[:, :128], 0.0).astype(bf16)
+        within_kappa = jnp.where(inclusive, pairs[:, 128:], 0.0).astype(bf16)
+        drop = pick(dot(within_beta, z_v[g]))
+        reads_v[g] = rho * end_of(0, g) - drop[:, :128]
+        local = pick(dot(within_kappa, part(2, *groups[g]))) - drop[:, 128:]
+        local_v[g] = local - head_mean(local)
     def send_state(j):
         return pltpu.make_async_remote_copy(
             src_ref=state_v.at[j],
@@ -463,38 +464,8 @@
     @pl.when(is_owner)
     def _():
         pltpu.make_async_copy(init_v, init_in, init_recv).wait()
-        start_state = cat([init_in[0], init_in[1]], 1)
-        for j in range(N_SP - 1):
-            wait_map(j)
-        zero = jnp.zeros((HD, 128), f32)
-
-        def then(left, transit, written):
-            return after_given(left, transit) + cat([zero, written.astype(f32)], 0)
-
-        def apply(state, held):
-            return after(state, held[:HD], held[HD:])
-
-        prefixes = []
-        for block in range(4):
-            prefixes.append([cat([maps_in[4 * block, 0], maps_in[4 * block, 1]], 0).astype(f32)])
-        for y in (1, 2, 3):
-            for block in range(4):
-                j = 4 * block + y
-                if j < N_SP - 1:
-                    prefixes[block].append(then(prefixes[block][-1], maps_in[j, 0], maps_in[j, 1]))
-        totals = [prefixes[block][3] for block in range(3)]
-        ahead = after(totals[1], totals[2][:HD], cat([zero, totals[2][HD:]], 0))
-        fourth = apply(start_state, totals[0])
-        starts = [start_state, fourth, apply(fourth, totals[1]), apply(fourth, ahead)]
-        for block in range(4):
-            state_v[4 * block] = centred(starts[block])
-            for y in (1, 2, 3):
-                inside = prefixes[block][y - 1]
-                moved = after_given(starts[block], inside[:HD].astype(bf16)) + inside[HD:]
-                state_v[4 * block + y] = centred(moved)
-
-        @pl.loop(0, N_SP)
-        def _(j):
+        state = cat([init_in[0], init_in[1]], 1)
+        def emit(j):
             @pl.when((j != sp) | (side == 0))
             def _():
                 send_state(j).start()
@@ -505,19 +476,20 @@
                     state_v.at[j], states_in.at[group_of], st_recv.at[group_of]
                 ).start()
 
-    late(0, slice(4, 6), slice(OFFS[0], OFFS[6]))
+        state_v[0] = centred(state)
+        emit(0)
+        for block in (range(0, 4), range(4, 8), range(8, 12), range(12, 14), range(14, 15)):
+            for j in block:
+                wait_map(j)
+            for j in block:
+                state = after_given(state, maps_in[j, 0]) + maps_in[j, 1].astype(f32)
+                state_v[j + 1] = centred(state)
+            for j in block:
+                emit(j + 1)
+
+    late(5, slice(5, 6), slice(OFFS[5], OFFS[6]))
     for copy in small[4:7] + small[8:]:
         copy.wait()
-
-    for g in every:
-        rho = part(0, *groups[g]).astype(f32) * pair_of(1, g)
-        pairs = pair_products(rho, turn_v[g, 0], turn_v[g, 1])
-        within_beta = jnp.where(inclusive, pairs[:, :128], 0.0).astype(bf16)
-        within_kappa = jnp.where(inclusive, pairs[:, 128:], 0.0).astype(bf16)
-        drop = pick(dot(within_beta, z_v[g]))
-        reads_v[g] = rho * end_of(0, g) - drop[:, :128]
-        local = pick(dot(within_kappa, part(2, *groups[g]))) - drop[:, 128:]
-        local_v[g] = local - head_mean(local)
     for b in range(SEQ):
         gate = rows_of(5, b)
         gate_v[b] = local_row(2) * (gate * sig(gate))

time: 30 us -> 28.6 us (0.953)
  Pallas kernels: 27.7 us -> 26.2 us
    pallas_call x1, Pallas kernels: 27.7 us -> 26.2 us  [shards(): pl.pallas_call(kernel, out_shape=[jax.ShapeDtypeStruct((SEQ, ROWS, HALF),...]
where the time goes in v5:
time: 28.6 us; the launch traced here: 28.4 us
  Pallas kernels  26.2 us (92%)
  other arithmetic  2.19 us (8%)
    pallas_call x1, Pallas kernels, shards(): pl.pallas_call(kernel, out_shape=[jax.ShapeDtypeStruct((SEQ, ROWS, HALF),...  26.2 us
    convert_element_type x1, other arithmetic, shards(): return (own.astype(f32) + arrived.astype(f32)).astype(bf16)  2.19 us

profile of v5, /device:TPU:1, one launch (start us, length us, event | category | flops | bytes accessed | tf_op | source)
XLA Modules:
  0.0 28.4 jit_solution(15877878519730704732)
XLA Ops:
  0.0 26.2 %layer.1 = (bf16[2,128,1024]{2,1,0:T(8,128)(2,1)}, bf16[2,128,1024]{2,1,0:T(8,128)(2,1)}) custom-call(bf16[2,128,1024]{2,1,0:T(8,128)(2,1)} %tok.1, f32[1,2048]{1,0:T(1,128)} %bitcast.5, bf16[2048,384]{1,0:T(8,128)(2,1)} %wr.1, bf16[2048,384]{1,0:T(8,128)(2,1)} %wk.1, bf16[2048,384]{1,0:T(8,128)(2,1)} %wv.1, bf16[2048,384]{1,0:T(8,128)(2,1)} %wd.1, ...), custom_call_target="tpu_custom_call" | custom-call | tf_op jit(solution)/shard_map/layer/pallas_call | solution.py:647
  26.2 2.2 %add_convert_fusion = bf16[2,128,1024]{2,1,0:T(8,128)(2,1)} fusion(bf16[2,128,1024]{2,1,0:T(8,128)(2,1)} %get-tuple-element.8, bf16[2,128,1024]{2,1,0:T(8,128)(2,1)} %get-tuple-element.7), kind=kLoop, calls=%fused_computation | loop fusion | flops 1048576 | bytes 1572864 | tf_op jit(solution)/shard_map/convert_element_type | solution.py:662

commit v6 on v5

--- a/solution.py
+++ b/solution.py
@@ -180,9 +180,9 @@
     own_out, arrived_out,
     tok_v, gain_v, weight_v, acc_v, proj_v, norm_v, square_v, base_v, mix_v, pscale_v, wout_v, init_v, init_in,
     scale_v, pool_v, keys_v, turn_v, low_v, side_v, z_v, reads_v, local_v, map_v, maps_in,
-    gate_v, state_v, states_in, merged_v, recout_v, part_v, part_own,
+    gate_v, state_v, states_in, merged_v, recout_v, part_v,
     w_sem, small_sem, tok_send, tok_recv, halo_send, halo_recv, map_send, map_recv,
-    st_send, st_recv, part_send, part_recv, own_sem, init_send, init_recv, pair_sem, go_sem,
+    st_send, st_recv, part_send, part_recv, init_send, init_recv, pair_sem, go_sem,
 ):
     sp = lax.axis_index("sp")
     tp = lax.axis_index("tp")
@@ -548,15 +548,12 @@
             device_id_type=MESH,
         )
 
-    def keep_part(tile):
-        return pltpu.make_async_copy(part_own.at[tile], columns(own_out, tile), own_sem.at[tile])
-
     for tile in range(2):
         part_v[tile] = product(pl.ds(pl.multiple_of(theirs + tile * 512, 512), 512))
         send_part(tile).start()
     for tile in range(2):
-        part_own[tile] = product(pl.ds(pl.multiple_of(mine + tile * 512, 512), 512))
-        keep_part(tile).start()
+        at = pl.ds(pl.multiple_of(mine + tile * 512, 512), 512)
+        own_out[:, :, 512 * tile : 512 * tile + 512] = product(at)
 
     for copy in send_tok:
         copy.wait_send()
@@ -584,7 +581,6 @@
 
     for tile in range(2):
         send_part(tile).wait()
-        keep_part(tile).wait()
 
 
 def shards(
@@ -625,7 +621,6 @@
         vmem((TOK, D), f32),
         vmem((TOK, RCOLS + PCOLS), bf16),
         vmem((2, SEQ, ROWS, 512), bf16),
-        vmem((2, SEQ, ROWS, 512), bf16),
         sem((2, 8)),
         sem((10,)),
         sem((2,)),
@@ -638,27 +633,27 @@
         sem((GROUPS,)),
         sem((2,)),
         sem((2,)),
-        sem((2,)),
         sem,
         sem,
         pltpu.SemaphoreType.REGULAR,
         pltpu.SemaphoreType.REGULAR,
     ]
+    pin = lambda x: pltpu.with_memory_space_constraint(x, pltpu.HBM)
     own, arrived = pl.pallas_call(
         kernel,
         out_shape=[jax.ShapeDtypeStruct((SEQ, ROWS, HALF), bf16)] * 2,
         in_specs=[pl.BlockSpec(memory_space=pl.ANY)] * 18,
-        out_specs=[pl.BlockSpec(memory_space=pl.ANY)] * 2,
+        out_specs=[pl.BlockSpec(memory_space=pltpu.VMEM)] * 2,
         scratch_shapes=scratch,
         compiler_params=pltpu.CompilerParams(
-            collective_id=0, has_side_effects=True, vmem_limit_bytes=56 << 20
+            collective_id=0, has_side_effects=True, vmem_limit_bytes=48 << 20
         ),
         name="layer",
-    )(
+    )(*(pin(x) for x in (
         tokens, row(norm_gain), w_recept, w_key, w_value, w_decay, w_rate, w_gate_rec, w_pool,
         w_gate_pool, tile(decay_base), tile(rate_base), tile(head_gain), pool_mix, row(pool_scale),
         w_out_rec, w_out_pool, init_state,
-    )
+    )))
     return (own.astype(f32) + arrived.astype(f32)).astype(bf16)
 
 

time: 28.6 us -> 27.1 us (0.948)
  other arithmetic: 2.19 us -> 0.99 us
    convert_element_type x1, other arithmetic: 2.19 us -> 0.99 us  [shards(): return (own.astype(f32) + arrived.astype(f32)).astype(bf16)]
where the time goes in v6:
time: 27.1 us; the launch traced here: 27 us
  Pallas kernels  26 us (96%)
  other arithmetic  0.99 us (4%)
    pallas_call x1, Pallas kernels, shards(): pl.pallas_call(kernel, out_shape=[jax.ShapeDtypeStruct((SEQ, ROWS, HALF),...  26 us
    convert_element_type x1, other arithmetic, shards(): return (own.astype(f32) + arrived.astype(f32)).astype(bf16)  0.99 us

profile of v6, /device:TPU:1, one launch (start us, length us, event | category | flops | bytes accessed | tf_op | source)
XLA Modules:
  0.0 27.0 jit_solution(2891569128383736193)
XLA Ops:
  0.0 26.0 %layer.1 = (bf16[2,128,1024]{2,1,0:T(8,128)(2,1)S(1)}, bf16[2,128,1024]{2,1,0:T(8,128)(2,1)S(1)}) custom-call(bf16[2,128,1024]{2,1,0:T(8,128)(2,1)} %tok.1, f32[1,2048]{1,0:T(1,128)} %bitcast.5, bf16[2048,384]{1,0:T(8,128)(2,1)} %wr.1, bf16[2048,384]{1,0:T(8,128)(2,1)} %wk.1, bf16[2048,384]{1,0:T(8,128)(2,1)} %wv.1, bf16[2048,384]{1,0:T(8,128)(2,1)} %wd.1, ...), custom_call_target="tpu_custom_call" | custom-call | tf_op jit(solution)/shard_map/layer/pallas_call | solution.py:642
  26.0 1.0 %add_convert_fusion = bf16[2,128,1024]{2,1,0:T(8,128)(2,1)} fusion(bf16[2,128,1024]{2,1,0:T(8,128)(2,1)S(1)} %get-tuple-element.8, bf16[2,128,1024]{2,1,0:T(8,128)(2,1)S(1)} %get-tuple-element.7), kind=kLoop, calls=%fused_computation | loop fusion | flops 1048576 | bytes 1572864 | tf_op jit(solution)/shard_map/convert_element_type | solution.py:657

commit v7 on v6

--- a/solution.py
+++ b/solution.py
@@ -105,10 +105,10 @@
     return alpha, shrink, beta, kappa, jnp.exp(mid), jnp.exp(last - mid), jnp.exp(last)
 
 
-def pair_products(x, y_hi, y_lo):
+def pair_products(x, turned):
     parts = [split2(keep(x, head)) for head in (0, 1)]
     lhs = cat([cat([hi, lo], 1) for hi, lo in parts], 0)
-    return dot(lhs, cat([y_hi, y_hi], 0)) + dot(lhs[:, :128], y_lo)
+    return dot(lhs, cat([turned, turned], 0))
 
 
 def pick(x):
@@ -120,19 +120,39 @@
     i = lax.broadcasted_iota(jnp.int32, (128, 128), 0)
     j = lax.broadcasted_iota(jnp.int32, (128, 128), 1)
     apart = i ^ j
-    eye = jnp.where(i == j, 1.0, 0.0)
+    same = apart < 32
     zero = jnp.zeros((128, 128), bf16)
-    inv = [eye - jnp.where(apart == 1, low, zero).astype(f32) for low in lowers]
-    for size in (2, 8, 32):
+
+    def packed(x):
+        return (x[:32] + x[32:64]) + (x[64:96] + x[96:])
+
+    def spread(x):
+        return jnp.where(same, cat([x] * 4, 0), jnp.zeros((128, 128), x.dtype))
+
+    eye = packed(jnp.where(i == j, 1.0, 0.0))
+    inv = [eye - packed(jnp.where(apart == 1, low, zero).astype(f32)) for low in lowers]
+    for size in (2, 8):
         inside = (apart >= size) & (apart < 4 * size)
         inv_b = [x.astype(bf16) for x in inv]
         hop = [
             dot(x, jnp.where(inside, low, zero)).astype(bf16) for x, low in zip(inv_b, lowers)
         ]
-        both = [dot(h, cat([h, x], 1)) for h, x in zip(hop, inv_b)]
+        both = [dot(h, cat([spread(h), spread(x)], 1)) for h, x in zip(hop, inv_b)]
         once = [x - y[:, 128:] for x, y in zip(inv, both)]
-        inv = [x + dot(y[:, :128].astype(bf16), x.astype(bf16)) for x, y in zip(once, both)]
-    return [x.astype(bf16) for x in inv]
+        inv = [
+            x + dot(y[:, :128].astype(bf16), spread(x.astype(bf16))) for x, y in zip(once, both)
+        ]
+    inv = [spread(x) for x in inv]
+    inv_b = [x.astype(bf16) for x in inv]
+    outside = apart >= 32
+    top = jnp.zeros((32, 128), bf16)
+    hop = [
+        dot(x[32:], jnp.where(outside, low, zero)).astype(bf16) for x, low in zip(inv_b, lowers)
+    ]
+    both = [dot(h, cat([cat([top, h], 0), x], 1)) for h, x in zip(hop, inv_b)]
+    once = [cat([x[:32], x[32:] - y[:, 128:]], 0) for x, y in zip(inv, both)]
+    last = [dot(y[32:, :128].astype(bf16), x.astype(bf16)) for x, y in zip(once, both)]
+    return [cat([x[:64], x[64:] + y], 0).astype(bf16) for x, y in zip(once, last)]
 
 
 def solve_all(invs, lows, sides):
@@ -340,11 +360,9 @@
 
     every = range(GROUPS)
     for g in every:
-        turned = cat([pair_of(2, g).T, pair_of(3, g).T], 1)
-        y_hi, y_lo = split2(turned)
-        turn_v[g, 0] = y_hi
-        turn_v[g, 1] = y_lo
-        pairs = pair_products(pair_of(0, g), y_hi, y_lo)
+        turned = cat([pair_of(2, g).astype(bf16).T, pair_of(3, g).astype(bf16).T], 1)
+        turn_v[g] = turned
+        pairs = pair_products(pair_of(0, g), turned)
         low_v[g] = jnp.where(strict, pairs[:, :128], 0.0).astype(bf16)
         cross = jnp.where(strict, pairs[:, 128:], 0.0).astype(bf16)
         side_v[g, :, :128] = pair_of(0, g) * end_of(0, g)
@@ -420,7 +438,7 @@
     late(0, slice(4, 5), slice(OFFS[0], OFFS[5]))
     for g in every:
         rho = part(0, *groups[g]).astype(f32) * pair_of(1, g)
-        pairs = pair_products(rho, turn_v[g, 0], turn_v[g, 1])
+        pairs = pair_products(rho, turn_v[g])
         within_beta = jnp.where(inclusive, pairs[:, :128], 0.0).astype(bf16)
         within_kappa = jnp.where(inclusive, pairs[:, 128:], 0.0).astype(bf16)
         drop = pick(dot(within_beta, z_v[g]))
@@ -470,12 +488,6 @@
             def _():
                 send_state(j).start()
 
-            @pl.when((j == sp) & (side == 1))
-            def _():
-                pltpu.make_async_copy(
-                    state_v.at[j], states_in.at[group_of], st_recv.at[group_of]
-                ).start()
-
         state_v[0] = centred(state)
         emit(0)
         for block in (range(0, 4), range(4, 8), range(8, 12), range(12, 14), range(14, 15)):
@@ -486,6 +498,12 @@
                 state_v[j + 1] = centred(state)
             for j in block:
                 emit(j + 1)
+
+        @pl.when(side == 1)
+        def _():
+            pltpu.make_async_copy(
+                state_v.at[sp], states_in.at[group_of], st_recv.at[group_of]
+            ).start()
 
     late(5, slice(5, 6), slice(OFFS[5], OFFS[6]))
     for copy in small[4:7] + small[8:]:
@@ -607,7 +625,7 @@
         vmem((TOK, 128), f32),
         vmem((SEQ, 16 + ROWS, PCOLS), bf16),
         vmem((SEQ, 4, ROWS, RCOLS), f32),
-        vmem((GROUPS, 2, 128, 256), bf16),
+        vmem((GROUPS, 128, 256), bf16),
         vmem((GROUPS, 256, 128), bf16),
         vmem((GROUPS, 128, 256), f32),
         vmem((GROUPS, 128, 256), bf16),

time: 27.1 us -> 26 us (0.959)
  Pallas kernels: 26 us -> 24.9 us
    pallas_call x1, Pallas kernels: 26 us -> 24.9 us  [shards(): pl.pallas_call(kernel, out_shape=[jax.ShapeDtypeStruct((SEQ, ROWS, HALF),...]
where the time goes in v7:
time: 26 us; the launch traced here: 25.9 us
  Pallas kernels  24.9 us (96%)
  other arithmetic  0.99 us (4%)
    pallas_call x1, Pallas kernels, shards(): pl.pallas_call(kernel, out_shape=[jax.ShapeDtypeStruct((SEQ, ROWS, HALF),...  24.9 us
    convert_element_type x1, other arithmetic, shards(): return (own.astype(f32) + arrived.astype(f32)).astype(bf16)  0.99 us

profile of v7, /device:TPU:1, one launch (start us, length us, event | category | flops | bytes accessed | tf_op | source)
XLA Modules:
  0.0 25.9 jit_solution(16128365131355828429)
XLA Ops:
  0.0 24.9 %layer.1 = (bf16[2,128,1024]{2,1,0:T(8,128)(2,1)S(1)}, bf16[2,128,1024]{2,1,0:T(8,128)(2,1)S(1)}) custom-call(bf16[2,128,1024]{2,1,0:T(8,128)(2,1)} %tok.1, f32[1,2048]{1,0:T(1,128)} %bitcast.5, bf16[2048,384]{1,0:T(8,128)(2,1)} %wr.1, bf16[2048,384]{1,0:T(8,128)(2,1)} %wk.1, bf16[2048,384]{1,0:T(8,128)(2,1)} %wv.1, bf16[2048,384]{1,0:T(8,128)(2,1)} %wd.1, ...), custom_call_target="tpu_custom_call" | custom-call | tf_op jit(solution)/shard_map/layer/pallas_call | solution.py:660
  24.9 1.0 %add_convert_fusion = bf16[2,128,1024]{2,1,0:T(8,128)(2,1)} fusion(bf16[2,128,1024]{2,1,0:T(8,128)(2,1)S(1)} %get-tuple-element.8, bf16[2,128,1024]{2,1,0:T(8,128)(2,1)S(1)} %get-tuple-element.7), kind=kLoop, calls=%fused_computation | loop fusion | flops 1048576 | bytes 1572864 | tf_op jit(solution)/shard_map/convert_element_type | solution.py:675

commit v8 on v7

--- a/solution.py
+++ b/solution.py
@@ -22,6 +22,7 @@
 OFFS = (1536, 0, 1152, 384, 768, 1920, 2304, 2560)
 NEED = (1, 3, 4, 2, 0, 5, 6, 7)
 EARLY = 4 * RCOLS
+OWNERS = ((0, 2, 4, 6, 8, 10), (1, 3, 5, 7, 9, 11))
 WIDTHS = (384, 384, 384, 384, 384, 384, 256, 256)
 MESH = pl.DeviceIdType.MESH
 f32 = jnp.float32
@@ -208,11 +209,18 @@
     tp = lax.axis_index("tp")
     other = 1 - tp
     weights = (wr, wk, wv, wd, wa, wg, wp, wgp)
-    group_of = lax.div(sp, 2)
-    side = lax.rem(sp, 2)
-    is_owner = (tp == 1) & (sp < 2 * GROUPS)
-    gives_init = (tp == 0) & (side == 0) & (sp < 2 * GROUPS)
-    keeps_init = (tp == 1) & (side == 1) & (sp < 2 * GROUPS)
+    group_of, side, owning = 0, 0, 0
+    for core in (0, 1):
+        for g, owner in enumerate(OWNERS[core]):
+            here = (sp == owner).astype(jnp.int32)
+            group_of, side, owning = group_of + here * g, side + here * core, owning + here
+    is_owner = (tp == 1) & (owning == 1)
+    gives_init = (tp == 0) & (side == 0) & (owning == 1)
+    keeps_init = (tp == 1) & (side == 1) & (owning == 1)
+
+    def owner_of(g):
+        return OWNERS[0][g] + tp * (OWNERS[1][g] - OWNERS[0][g])
+
 
     barrier = pltpu.get_barrier_semaphore()
 
@@ -226,7 +234,7 @@
     mine = pl.multiple_of(tp * HALF, HALF)
     theirs = pl.multiple_of(other * HALF, HALF)
     pool_at = pl.multiple_of(tp * PCOLS, 128)
-    held = jnp.minimum(group_of, GROUPS - 1)
+    held = group_of
     small = [
         pltpu.make_async_copy(tok, tok_v, small_sem.at[0]),
         pltpu.make_async_copy(gain.at[:, pl.ds(mine, HALF)], gain_v, small_sem.at[1]),
@@ -339,6 +347,24 @@
     def local_row(index):
         return cat([base_v[index, pl.ds(3 * tp + p, 1), :] for p in range(PAIRS)], 1)
 
+    small[7].wait()
+    give = pltpu.make_async_remote_copy(
+        src_ref=init_v,
+        dst_ref=init_in,
+        send_sem=init_send,
+        recv_sem=init_recv,
+        device_id={"tp": other},
+        device_id_type=MESH,
+    )
+
+    @pl.when(gives_init)
+    def _():
+        give.start()
+
+    @pl.when(keeps_init)
+    def _():
+        pltpu.make_async_copy(init_v, init_in, init_recv).start()
+
     ends = []
     for b in range(SEQ):
         alpha, shrink, beta, kappa, e_mid, e_tail, e_last = prepare(
@@ -388,14 +414,14 @@
     def _():
         pl.semaphore_wait(go_sem, 1)
 
-    own_map = [(tp == 1) & (sp == 2 * g + 1) for g in every]
+    own_map = [(tp == 1) & (sp == OWNERS[1][g]) for g in every]
     for g in every:
         copy = pltpu.make_async_remote_copy(
             src_ref=map_v.at[g],
             dst_ref=maps_in.at[sp],
             send_sem=map_send.at[g],
             recv_sem=map_recv.at[sp],
-            device_id={"sp": 2 * g + tp, "tp": 1},
+            device_id={"sp": owner_of(g), "tp": 1},
             device_id_type=MESH,
         )
         map_copies.append(copy)
@@ -407,6 +433,33 @@
         @pl.when(own_map[g])
         def _():
             pltpu.make_async_copy(map_v.at[g], maps_in.at[sp], map_recv.at[sp]).start()
+
+    def send_state(j):
+        return pltpu.make_async_remote_copy(
+            src_ref=state_v.at[j],
+            dst_ref=states_in.at[group_of],
+            send_sem=st_send.at[j],
+            recv_sem=st_recv.at[group_of],
+            device_id={"sp": j, "tp": side},
+            device_id_type=MESH,
+        )
+
+    def wait_map(j):
+        pltpu.make_async_copy(map_v.at[0], maps_in.at[j], map_recv.at[j]).wait()
+
+    def centred(state):
+        return (state - jnp.mean(state, axis=0, keepdims=True)).astype(bf16)
+
+    def emit(j):
+        @pl.when((j != sp) | (side == 0))
+        def _():
+            send_state(j).start()
+
+    @pl.when(is_owner)
+    def _():
+        pltpu.make_async_copy(init_v, init_in, init_recv).wait()
+        state_v[0] = centred(cat([init_in[0], init_in[1]], 1))
+        emit(0)
 
     def late(index, copies, at):
         for half in (0, 1):
@@ -445,52 +498,49 @@
         reads_v[g] = rho * end_of(0, g) - drop[:, :128]
         local = pick(dot(within_kappa, part(2, *groups[g]))) - drop[:, 128:]
         local_v[g] = local - head_mean(local)
-    def send_state(j):
-        return pltpu.make_async_remote_copy(
-            src_ref=state_v.at[j],
-            dst_ref=states_in.at[group_of],
-            send_sem=st_send.at[j],
-            recv_sem=st_recv.at[group_of],
-            device_id={"sp": j, "tp": side},
-            device_id_type=MESH,
-        )
-
-    def wait_map(j):
-        pltpu.make_async_copy(map_v.at[0], maps_in.at[j], map_recv.at[j]).wait()
-
-    def centred(state):
-        return (state - jnp.mean(state, axis=0, keepdims=True)).astype(bf16)
-
-    small[7].wait()
-    give = pltpu.make_async_remote_copy(
-        src_ref=init_v,
-        dst_ref=init_in,
-        send_sem=init_send,
-        recv_sem=init_recv,
-        device_id={"tp": other},
-        device_id_type=MESH,
-    )
-
-    @pl.when(gives_init)
-    def _():
-        give.start()
-
-    @pl.when(keeps_init)
-    def _():
-        pltpu.make_async_copy(init_v, init_in, init_recv).start()
+    def late_work():
+        late(5, slice(5, 6), slice(OFFS[5], OFFS[6]))
+        for copy in small[4:7] + small[8:]:
+            copy.wait()
+        for b in range(SEQ):
+            gate = rows_of(5, b)
+            gate_v[b] = local_row(2) * (gate * sig(gate))
+
+        @pl.when(sp > 0)
+        def _():
+            halo.wait_recv()
+
+        places = (sp * ROWS + 1 + lax.broadcasted_iota(jnp.int32, (ROWS, 128), 0)).astype(f32)
+        for b in range(SEQ):
+            outs = []
+            for s in range(2):
+                at = slice(128 * s, 128 * s + 128)
+                own = pool_v[b, :, at].astype(f32)
+                total = own + pltpu.roll(own, 1, 0)
+                if s == 1:
+                    total = total + pltpu.roll(total, 2, 0)
+                wide = total + pltpu.roll(total, 2 if s == 0 else 4, 0)
+                wide = wide + pltpu.roll(wide, 4 if s == 0 else 8, 0)
+                trail = jnp.where(tp == 0, total, wide)[16:]
+                window = jnp.where(tp == 0, float(2 << s), float(8 << s))
+                diff = (trail / jnp.minimum(places, window) - own[16:]).astype(bf16)
+                pooled = dot(diff, mix_v[s])
+                gate = proj_v[b * ROWS : (b + 1) * ROWS, OFFS[7] + 128 * s : OFFS[7] + 128 * s + 128]
+                gate = gate.astype(f32)
+                outs.append((pooled * pscale_v[:, at] * (gate * sig(gate))).astype(bf16))
+            recout_v[b * ROWS : (b + 1) * ROWS, RCOLS:] = cat(outs, 1)
+
+        for at in (slice(0, 1024), slice(1024, D)):
+            merged_v[:, at] = dot(recout_v[:, RCOLS:], wout_v[RCOLS:, at])
+
+    @pl.when(sp < 8)
+    def _():
+        late_work()
 
     @pl.when(is_owner)
     def _():
-        pltpu.make_async_copy(init_v, init_in, init_recv).wait()
         state = cat([init_in[0], init_in[1]], 1)
-        def emit(j):
-            @pl.when((j != sp) | (side == 0))
-            def _():
-                send_state(j).start()
-
-        state_v[0] = centred(state)
-        emit(0)
-        for block in (range(0, 4), range(4, 8), range(8, 12), range(12, 14), range(14, 15)):
+        for block in ((0,), (1,), (2,), (3,), (4, 5), (6, 7), (8, 9), (10, 11), (12,), (13,), (14,)):
             for j in block:
                 wait_map(j)
             for j in block:
@@ -505,39 +555,9 @@
                 state_v.at[sp], states_in.at[group_of], st_recv.at[group_of]
             ).start()
 
-    late(5, slice(5, 6), slice(OFFS[5], OFFS[6]))
-    for copy in small[4:7] + small[8:]:
-        copy.wait()
-    for b in range(SEQ):
-        gate = rows_of(5, b)
-        gate_v[b] = local_row(2) * (gate * sig(gate))
-
-    @pl.when(sp > 0)
-    def _():
-        halo.wait_recv()
-
-    places = (sp * ROWS + 1 + lax.broadcasted_iota(jnp.int32, (ROWS, 128), 0)).astype(f32)
-    for b in range(SEQ):
-        outs = []
-        for s in range(2):
-            at = slice(128 * s, 128 * s + 128)
-            own = pool_v[b, :, at].astype(f32)
-            total = own + pltpu.roll(own, 1, 0)
-            if s == 1:
-                total = total + pltpu.roll(total, 2, 0)
-            wide = total + pltpu.roll(total, 2 if s == 0 else 4, 0)
-            wide = wide + pltpu.roll(wide, 4 if s == 0 else 8, 0)
-            trail = jnp.where(tp == 0, total, wide)[16:]
-            window = jnp.where(tp == 0, float(2 << s), float(8 << s))
-            diff = (trail / jnp.minimum(places, window) - own[16:]).astype(bf16)
-            pooled = dot(diff, mix_v[s])
-            gate = proj_v[b * ROWS : (b + 1) * ROWS, OFFS[7] + 128 * s : OFFS[7] + 128 * s + 128]
-            gate = gate.astype(f32)
-            outs.append((pooled * pscale_v[:, at] * (gate * sig(gate))).astype(bf16))
-        recout_v[b * ROWS : (b + 1) * ROWS, RCOLS:] = cat(outs, 1)
-
-    for at in (slice(0, 1024), slice(1024, D)):
-        merged_v[:, at] = dot(recout_v[:, RCOLS:], wout_v[RCOLS:, at])
+    @pl.when(sp >= 8)
+    def _():
+        late_work()
 
     for g in every:
         pltpu.make_async_copy(state_v.at[0], states_in.at[g], st_recv.at[g]).wait()

time: 26 us -> 24.5 us (0.942)
  the two profiles are of different devices: /device:TPU:1 before, /device:TPU:101 now
where the time goes in v8:
time: 24.5 us; the launch traced here: 24.4 us
  Pallas kernels  23.4 us (96%)
  other arithmetic  0.99 us (4%)
    pallas_call x1, Pallas kernels, shards(): pl.pallas_call(kernel, out_shape=[jax.ShapeDtypeStruct((SEQ, ROWS, HALF),...  23.4 us
    convert_element_type x1, other arithmetic, shards(): return (own.astype(f32) + arrived.astype(f32)).astype(bf16)  0.99 us

profile of v8, /device:TPU:101, one launch (start us, length us, event | category | flops | bytes accessed | tf_op | source)
XLA Modules:
  0.0 24.4 jit_solution(14428484869881963956)
XLA Ops:
  0.0 23.4 %layer.1 = (bf16[2,128,1024]{2,1,0:T(8,128)(2,1)S(1)}, bf16[2,128,1024]{2,1,0:T(8,128)(2,1)S(1)}) custom-call(bf16[2,128,1024]{2,1,0:T(8,128)(2,1)} %tok.1, f32[1,2048]{1,0:T(1,128)} %bitcast.5, bf16[2048,384]{1,0:T(8,128)(2,1)} %wr.1, bf16[2048,384]{1,0:T(8,128)(2,1)} %wk.1, bf16[2048,384]{1,0:T(8,128)(2,1)} %wv.1, bf16[2048,384]{1,0:T(8,128)(2,1)} %wd.1, ...), custom_call_target="tpu_custom_call" | custom-call | tf_op jit(solution)/shard_map/layer/pallas_call | solution.py:680
  23.4 1.0 %add_convert_fusion = bf16[2,128,1024]{2,1,0:T(8,128)(2,1)} fusion(bf16[2,128,1024]{2,1,0:T(8,128)(2,1)S(1)} %get-tuple-element.8, bf16[2,128,1024]{2,1,0:T(8,128)(2,1)S(1)} %get-tuple-element.7), kind=kLoop, calls=%fused_computation | loop fusion | flops 1048576 | bytes 1572864 | tf_op jit(solution)/shard_map/convert_element_type | solution.py:695

commit v9 on v8

--- a/solution.py
+++ b/solution.py
@@ -276,12 +276,13 @@
         pl.semaphore_wait(barrier, 1)
         tell(pair_sem, tp=other)
 
-    start(loads[0][2:4] + loads[1][:4] + small[2:4])
+    start(loads[0][2:4])
     small[1].wait()
     wide = tok_v[...].reshape(TOK, HALF).astype(f32)
     norm_v[0] = (wide * gain_v[...]).astype(bf16)
     squares = wide * wide
     square_v[0] = sum(squares[:, o : o + 128] for o in range(0, HALF, 128))
+    start(loads[1][:4] + small[2:4])
 
     @pl.when(tp == 1)
     def _():
@@ -533,14 +534,14 @@
         for at in (slice(0, 1024), slice(1024, D)):
             merged_v[:, at] = dot(recout_v[:, RCOLS:], wout_v[RCOLS:, at])
 
-    @pl.when(sp < 8)
+    @pl.when(sp < 6)
     def _():
         late_work()
 
     @pl.when(is_owner)
     def _():
         state = cat([init_in[0], init_in[1]], 1)
-        for block in ((0,), (1,), (2,), (3,), (4, 5), (6, 7), (8, 9), (10, 11), (12,), (13,), (14,)):
+        for block in ((0,), (1,), (2,), (3,), (4, 5), (6, 7), (8,), (9,), (10,), (11,), (12,), (13,), (14,)):
             for j in block:
                 wait_map(j)
             for j in block:
@@ -555,7 +556,7 @@
                 state_v.at[sp], states_in.at[group_of], st_recv.at[group_of]
             ).start()
 
-    @pl.when(sp >= 8)
+    @pl.when(sp >= 6)
     def _():
         late_work()
 

time: 24.5 us -> 24.3 us (level)
  Pallas kernels: 23.4 us -> 23.1 us
    pallas_call x1, Pallas kernels: 23.4 us -> 23.1 us  [shards(): pl.pallas_call(kernel, out_shape=[jax.ShapeDtypeStruct((SEQ, ROWS, HALF),...]
where the time goes in v9:
time: 24.3 us; the launch traced here: 24.1 us
  Pallas kernels  23.1 us (95%)
  other arithmetic  0.99 us (4%)
    pallas_call x1, Pallas kernels, shards(): pl.pallas_call(kernel, out_shape=[jax.ShapeDtypeStruct((SEQ, ROWS, HALF),...  23.1 us
    convert_element_type x1, other arithmetic, shards(): return (own.astype(f32) + arrived.astype(f32)).astype(bf16)  0.99 us

profile of v9, /device:TPU:101, one launch (start us, length us, event | category | flops | bytes accessed | tf_op | source)
XLA Modules:
  0.0 24.1 jit_solution(12983555205994672235)
XLA Ops:
  0.0 23.1 %layer.1 = (bf16[2,128,1024]{2,1,0:T(8,128)(2,1)S(1)}, bf16[2,128,1024]{2,1,0:T(8,128)(2,1)S(1)}) custom-call(bf16[2,128,1024]{2,1,0:T(8,128)(2,1)} %tok.1, f32[1,2048]{1,0:T(1,128)} %bitcast.5, bf16[2048,384]{1,0:T(8,128)(2,1)} %wr.1, bf16[2048,384]{1,0:T(8,128)(2,1)} %wk.1, bf16[2048,384]{1,0:T(8,128)(2,1)} %wv.1, bf16[2048,384]{1,0:T(8,128)(2,1)} %wd.1, ...), custom_call_target="tpu_custom_call" | custom-call | tf_op jit(solution)/shard_map/layer/pallas_call | solution.py:681
  23.1 1.0 %add_convert_fusion = bf16[2,128,1024]{2,1,0:T(8,128)(2,1)} fusion(bf16[2,128,1024]{2,1,0:T(8,128)(2,1)S(1)} %get-tuple-element.8, bf16[2,128,1024]{2,1,0:T(8,128)(2,1)S(1)} %get-tuple-element.7), kind=kLoop, calls=%fused_computation | loop fusion | flops 1048576 | bytes 1572864 | tf_op jit(solution)/shard_map/convert_element_type | solution.py:696

commit v10 on v9

--- a/solution.py
+++ b/solution.py
@@ -386,14 +386,17 @@
         return ends[b][index][:, 128 * p : 128 * p + 128]
 
     every = range(GROUPS)
+    turns = [
+        cat([pair_of(2, g).astype(bf16).T, pair_of(3, g).astype(bf16).T], 1) for g in every
+    ]
+    products = [pair_products(pair_of(0, g), turns[g]) for g in every]
+    crosses = [jnp.where(strict, x[:, 128:], 0.0).astype(bf16) for x in products]
+    carried = [pick(dot(x, part(2, *groups[g]))) for g, x in zip(every, crosses)]
     for g in every:
-        turned = cat([pair_of(2, g).astype(bf16).T, pair_of(3, g).astype(bf16).T], 1)
-        turn_v[g] = turned
-        pairs = pair_products(pair_of(0, g), turned)
-        low_v[g] = jnp.where(strict, pairs[:, :128], 0.0).astype(bf16)
-        cross = jnp.where(strict, pairs[:, 128:], 0.0).astype(bf16)
+        turn_v[g] = turns[g]
+        low_v[g] = jnp.where(strict, products[g][:, :128], 0.0).astype(bf16)
         side_v[g, :, :128] = pair_of(0, g) * end_of(0, g)
-        side_v[g, :, 128:] = pick(dot(cross, part(2, *groups[g])))
+        side_v[g, :, 128:] = carried[g]
     @pl.when(tp == 1)
     def _():
         pl.semaphore_wait(barrier, N_SP - 1)

time: 24.3 us -> 23.6 us (0.971)
  the two profiles are of different devices: /device:TPU:101 before, /device:TPU:33 now
where the time goes in v10:
time: 23.6 us; the launch traced here: 23.5 us
  Pallas kernels  22.5 us (95%)
  other arithmetic  0.99 us (4%)
    pallas_call x1, Pallas kernels, shards(): pl.pallas_call(kernel, out_shape=[jax.ShapeDtypeStruct((SEQ, ROWS, HALF),...  22.5 us
    convert_element_type x1, other arithmetic, shards(): return (own.astype(f32) + arrived.astype(f32)).astype(bf16)  0.99 us

profile of v10, /device:TPU:33, one launch (start us, length us, event | category | flops | bytes accessed | tf_op | source)
XLA Modules:
  0.0 23.5 jit_solution(665089791140322120)
XLA Ops:
  0.0 22.5 %layer.1 = (bf16[2,128,1024]{2,1,0:T(8,128)(2,1)S(1)}, bf16[2,128,1024]{2,1,0:T(8,128)(2,1)S(1)}) custom-call(bf16[2,128,1024]{2,1,0:T(8,128)(2,1)} %tok.1, f32[1,2048]{1,0:T(1,128)} %bitcast.5, bf16[2048,384]{1,0:T(8,128)(2,1)} %wr.1, bf16[2048,384]{1,0:T(8,128)(2,1)} %wk.1, bf16[2048,384]{1,0:T(8,128)(2,1)} %wv.1, bf16[2048,384]{1,0:T(8,128)(2,1)} %wd.1, ...), custom_call_target="tpu_custom_call" | custom-call | tf_op jit(solution)/shard_map/layer/pallas_call | solution.py:684
  22.5 1.0 %add_convert_fusion = bf16[2,128,1024]{2,1,0:T(8,128)(2,1)} fusion(bf16[2,128,1024]{2,1,0:T(8,128)(2,1)S(1)} %get-tuple-element.8, bf16[2,128,1024]{2,1,0:T(8,128)(2,1)S(1)} %get-tuple-element.7), kind=kLoop, calls=%fused_computation | loop fusion | flops 1048576 | bytes 1572864 | tf_op jit(solution)/shard_map/convert_element_type | solution.py:699

commit v11 on v10

--- a/solution.py
+++ b/solution.py
@@ -493,15 +493,19 @@
         pool_v[:, 0:16, :] = jnp.zeros((SEQ, 16, PCOLS), bf16)
 
     late(0, slice(4, 5), slice(OFFS[0], OFFS[5]))
+    rhos = [part(0, *groups[g]).astype(f32) * pair_of(1, g) for g in every]
+    products = [pair_products(rho, turn_v[g]) for g, rho in zip(every, rhos)]
+    masked = [
+        [jnp.where(inclusive, x[:, o : o + 128], 0.0).astype(bf16) for o in (0, 128)]
+        for x in products
+    ]
+    drops = [pick(dot(masked[g][0], z_v[g])) for g in every]
+    adds = [pick(dot(masked[g][1], part(2, *groups[g]))) for g in every]
+    locals_ = [x - y[:, 128:] for x, y in zip(adds, drops)]
+    means = [head_mean(x) for x in locals_]
     for g in every:
-        rho = part(0, *groups[g]).astype(f32) * pair_of(1, g)
-        pairs = pair_products(rho, turn_v[g])
-        within_beta = jnp.where(inclusive, pairs[:, :128], 0.0).astype(bf16)
-        within_kappa = jnp.where(inclusive, pairs[:, 128:], 0.0).astype(bf16)
-        drop = pick(dot(within_beta, z_v[g]))
-        reads_v[g] = rho * end_of(0, g) - drop[:, :128]
-        local = pick(dot(within_kappa, part(2, *groups[g]))) - drop[:, 128:]
-        local_v[g] = local - head_mean(local)
+        reads_v[g] = rhos[g] * end_of(0, g) - drops[g][:, :128]
+        local_v[g] = locals_[g] - means[g]
     def late_work():
         late(5, slice(5, 6), slice(OFFS[5], OFFS[6]))
         for copy in small[4:7] + small[8:]:

time: 23.6 us -> 23.6 us (level)
  no operation moved by 1% of the time
where the time goes in v11:
time: 23.6 us; the launch traced here: 23.5 us
  Pallas kernels  22.5 us (95%)
  other arithmetic  0.99 us (4%)
    pallas_call x1, Pallas kernels, shards(): pl.pallas_call(kernel, out_shape=[jax.ShapeDtypeStruct((SEQ, ROWS, HALF),...  22.5 us
    convert_element_type x1, other arithmetic, shards(): return (own.astype(f32) + arrived.astype(f32)).astype(bf16)  0.99 us

profile of v11, /device:TPU:33, one launch (start us, length us, event | category | flops | bytes accessed | tf_op | source)
XLA Modules:
  0.0 23.5 jit_solution(9956667572558414599)
XLA Ops:
  0.0 22.5 %layer.1 = (bf16[2,128,1024]{2,1,0:T(8,128)(2,1)S(1)}, bf16[2,128,1024]{2,1,0:T(8,128)(2,1)S(1)}) custom-call(bf16[2,128,1024]{2,1,0:T(8,128)(2,1)} %tok.1, f32[1,2048]{1,0:T(1,128)} %bitcast.5, bf16[2048,384]{1,0:T(8,128)(2,1)} %wr.1, bf16[2048,384]{1,0:T(8,128)(2,1)} %wk.1, bf16[2048,384]{1,0:T(8,128)(2,1)} %wv.1, bf16[2048,384]{1,0:T(8,128)(2,1)} %wd.1, ...), custom_call_target="tpu_custom_call" | custom-call | tf_op jit(solution)/shard_map/layer/pallas_call | solution.py:688
  22.5 1.0 %add_convert_fusion = bf16[2,128,1024]{2,1,0:T(8,128)(2,1)} fusion(bf16[2,128,1024]{2,1,0:T(8,128)(2,1)S(1)} %get-tuple-element.8, bf16[2,128,1024]{2,1,0:T(8,128)(2,1)S(1)} %get-tuple-element.7), kind=kLoop, calls=%fused_computation | loop fusion | flops 1048576 | bytes 1572864 | tf_op jit(solution)/shard_map/convert_element_type | solution.py:703
